TPU v7x, 32 devices: a whole 2x2x4 slice. The times are simulated.
32 devices in a mesh: sp: 8 (over z, x), tp: 4 (over y, core).
Axes of the slice: x: 2, y: 2, z: 4, core: 2. Of those that a mesh axis runs over, the one named last changes fastest.
Arguments:
- tokens: bfloat16 [1024, 2048], P(('sp', 'tp')), may hold values from -6 to 6
- pre_gain: bfloat16 [2048], replicated, may hold values from 0.099609375 to 1.8984375
- w_query: bfloat16 [2048, 1024], P('sp', 'tp'), may hold values from -0.125 to 0.125
- w_key: bfloat16 [2048, 1024], P('sp', 'tp'), may hold values from -0.125 to 0.125
- w_value: bfloat16 [2048, 2048], P('sp', 'tp'), may hold values from -0.125 to 0.125
- w_igate: bfloat16 [2048, 8], replicated, may hold values from -1 to 1
- w_fgate: bfloat16 [2048, 8], replicated, may hold values from -0.125 to 0.125
- forget_bias: float32 [8], replicated, may hold values from 4 to 16
- gate_drift: float32 [1024, 8], P('sp'), may hold values from -2 to 2, as said below
- head_gain: bfloat16 [2048], replicated, may hold values from 0.099609375 to 1.8984375
- w_out: bfloat16 [2048, 2048], P('sp', 'tp'), may hold values from -0.125 to 0.125
Outputs:
- layer_out: bfloat16 [1024, 2048], P(('sp', 'tp'))
Inputs may be any that keep to these rules, and one draw needn't show every extreme that they name: `gate_drift`: constant over aligned spans of 128 positions.
All inputs are finite; a program needn't handle non-finite values.
Results may differ from a plain program's by a relative error of at most 0.02.
Values may be sent and summed in bfloat16 or wider, within the bound.
A program may use at most 64 MiB of HBM per device.

v0:
```python
import functools

import jax
import jax.numpy as jnp
from jax import lax
from jax.experimental import pallas as pl
from jax.experimental.pallas import tpu as pltpu
from jax.sharding import PartitionSpec as P

BLOCK = 64


norm_floor = 0.1
lowest_log = -1e30
highest = lax.Precision.HIGHEST


def prefix(value, axis, combine, identity):
    peers, position = (lax.axis_size(axis), lax.axis_index(axis))
    everything = jax.tree.map(
        lambda part, kind: lax.all_gather(part.astype(kind), axis),
        value,
        jax.tree.map(lambda a: jnp.bfloat16 if a.dtype == jnp.float32 else a.dtype, value),
    )
    start = jax.tree.map(
        lambda part, zero: jnp.broadcast_to(jnp.asarray(zero, part.dtype), part.shape),
        value,
        identity,
    )

    def step(k, before):
        reached = k < position
        new = combine(
            before, jax.tree.map(lambda part, own: part[k].astype(own.dtype), everything, value)
        )
        return jax.tree.map(lambda a, b: jnp.where(reached, a, b), new, before)

    return lax.fori_loop(0, peers, step, start)


def advance(memory, summary):
    old_mat, old_vec, old_top = memory
    span_log, span_top, span_mat, span_vec = summary
    new_top = jnp.maximum(span_log + old_top, span_top)
    kept_part = jnp.exp(span_log + old_top - new_top)
    fresh_part = jnp.exp(span_top - new_top)
    return (
        kept_part[:, None, None] * old_mat + fresh_part[:, None, None] * span_mat,
        kept_part[:, None] * old_vec + fresh_part[:, None] * span_vec,
        new_top,
    )


def prefix_states(initial, summary):

    def stepper(memory, one_block):
        return (advance(memory, one_block), memory)

    return lax.scan(stepper, initial, summary)


def join_devices(earlier, later_part):
    early_log, early_mat, early_vec, early_top = earlier
    late_log, late_mat, late_vec, late_top = later_part
    new_top = jnp.maximum(late_log + early_top, late_top)
    kept_part = jnp.exp(late_log + early_top - new_top)
    fresh_part = jnp.exp(late_top - new_top)
    return (
        early_log + late_log,
        kept_part[:, None, None] * early_mat + fresh_part[:, None, None] * late_mat,
        kept_part[:, None] * early_vec + fresh_part[:, None] * late_vec,
        new_top,
    )


def blend_parts(first_part, second_part):
    numer_first, denom_first, peak_first = first_part
    numer_second, denom_second, peak_second = second_part
    new_top = jnp.maximum(peak_first, peak_second)
    weight_first = jnp.exp(peak_first - new_top)
    weight_second = jnp.exp(peak_second - new_top)
    return (
        weight_first[..., None] * numer_first + weight_second[..., None] * numer_second,
        weight_first * denom_first + weight_second * denom_second,
        new_top,
    )


def on_device(
    tokens,
    pre_gain,
    w_query,
    w_key,
    w_value,
    w_igate,
    w_fgate,
    forget_bias,
    gate_drift,
    head_gain,
    w_out,
):
    tp_size = lax.axis_size("tp")
    head_count = w_igate.shape[1]
    local_heads = head_count // tp_size
    first_head = lax.axis_index("tp") * local_heads
    key_width = w_query.shape[1] // local_heads
    value_width = w_value.shape[1] // local_heads
    token_wide = tokens.astype(jnp.float32)
    scaled = token_wide * lax.rsqrt(
        jnp.mean(token_wide * token_wide, axis=1, keepdims=True) + norm_floor
    )
    normed = (scaled * pre_gain.astype(jnp.float32)).astype(jnp.bfloat16)
    gate_cols = jnp.concatenate(
        [
            lax.dynamic_slice_in_dim(w_igate, first_head, local_heads, 1),
            lax.dynamic_slice_in_dim(w_fgate, first_head, local_heads, 1),
        ],
        axis=1,
    )
    key_scale = key_width ** (-0.5)
    wq_full, wk_full, wv_full = (
        lax.all_gather(w_query, "sp", axis=0, tiled=True),
        lax.all_gather(w_key, "sp", axis=0, tiled=True),
        lax.all_gather(w_value, "sp", axis=0, tiled=True),
    )
    row_piece = lax.all_gather(normed, "tp", axis=0, tiled=True)
    queries_part = jnp.dot(row_piece, wq_full, preferred_element_type=jnp.float32).astype(
        jnp.bfloat16
    )
    keys_part = (
        jnp.dot(row_piece, wk_full, preferred_element_type=jnp.float32) * key_scale
    ).astype(jnp.bfloat16)
    values_part = jnp.dot(row_piece, wv_full, preferred_element_type=jnp.float32).astype(
        jnp.bfloat16
    )
    gate_part = jnp.dot(row_piece, gate_cols, preferred_element_type=jnp.float32)
    group_len = queries_part.shape[0]
    blocks = group_len // BLOCK
    log_input = gate_part[:, :local_heads]
    forget_pre = gate_part[:, local_heads:] + lax.dynamic_slice_in_dim(
        forget_bias, first_head, local_heads, 0
    )
    log_forget = jax.nn.log_sigmoid(
        forget_pre + lax.dynamic_slice_in_dim(gate_drift, first_head, local_heads, 1)
    )
    query_blk = queries_part.reshape(blocks, BLOCK, local_heads, key_width)
    key_blk = keys_part.reshape(blocks, BLOCK, local_heads, key_width)
    value_blk = values_part.reshape(blocks, BLOCK, local_heads, value_width)
    input_blk = log_input.reshape(blocks, BLOCK, local_heads).transpose(0, 2, 1)
    forget_blk = log_forget.reshape(blocks, BLOCK, local_heads).transpose(0, 2, 1)
    within = jnp.cumsum(forget_blk, axis=2)
    causal = jnp.arange(BLOCK)[:, None] >= jnp.arange(BLOCK)[None, :]
    log_pair = jnp.where(
        causal, within[..., :, None] - within[..., None, :] + input_blk[..., None, :], -jnp.inf
    )
    peak_intra = jnp.max(log_pair, axis=3)
    scores = jnp.einsum("nshd,nrhd->nhsr", query_blk, key_blk, preferred_element_type=jnp.float32)
    weights = scores * jnp.exp(log_pair - peak_intra[..., None])
    numer_intra = jnp.einsum(
        "nhsr,nrhv->nhsv",
        weights.astype(jnp.bfloat16),
        value_blk,
        preferred_element_type=jnp.float32,
    )
    denom_intra = jnp.sum(weights, axis=3)
    span_log = within[..., -1]
    log_write = span_log[..., None] - within + input_blk
    span_top = jnp.max(log_write, axis=2)
    write_scale = jnp.exp(log_write - span_top[..., None])
    key_scaled = key_blk.astype(jnp.float32) * write_scale.transpose(0, 2, 1)[..., None]
    value_wide = value_blk.astype(jnp.float32)
    span_mat = jnp.einsum("nrhv,nrhd->nhvd", value_wide, key_scaled, precision=highest)
    span_vec = jnp.sum(key_scaled, axis=1)
    summary = (span_log, span_top, span_mat, span_vec)
    empty_state = (
        jnp.zeros((local_heads, value_width, key_width), jnp.float32),
        jnp.zeros((local_heads, key_width), jnp.float32),
        jnp.full((local_heads,), lowest_log, jnp.float32),
    )
    local_end, local_starts = prefix_states(empty_state, summary)
    device_summary = (jnp.sum(span_log, axis=0),) + local_end
    identity_all = (jnp.zeros((local_heads,), jnp.float32),) + empty_state
    incoming = prefix(device_summary, "sp", join_devices, identity_all)
    query_wide = query_blk.astype(jnp.float32)
    intra_part = (numer_intra, denom_intra, peak_intra)
    start_mat, start_vec, start_top = local_starts
    local_part = (
        jnp.einsum("nhvd,nshd->nhsv", start_mat, query_wide, precision=highest),
        jnp.einsum("nhd,nshd->nhs", start_vec, query_wide, precision=highest),
        within + start_top[..., None],
    )
    numerator, denominator, peak_log = blend_parts(local_part, intra_part)
    entry_log, entry_mat, entry_vec, entry_top = incoming
    before_log = jnp.concatenate(
        [jnp.zeros((1, local_heads), jnp.float32), jnp.cumsum(span_log, axis=0)[:-1]], axis=0
    )
    from_left = (
        jnp.einsum("hvd,nshd->nhsv", entry_mat, query_wide, precision=highest),
        jnp.einsum("hd,nshd->nhs", entry_vec, query_wide, precision=highest),
        within + (before_log + entry_top[None, :])[..., None],
    )
    numerator, denominator, peak_log = blend_parts((numerator, denominator, peak_log), from_left)
    hidden = numerator / jnp.maximum(jnp.abs(denominator), jnp.exp(-peak_log))[..., None]
    hidden = hidden.transpose(0, 2, 1, 3).reshape(group_len, local_heads, value_width)
    head_gains = lax.dynamic_slice_in_dim(
        head_gain, first_head * value_width, local_heads * value_width, 0
    )
    head_gains = head_gains.astype(jnp.float32).reshape(local_heads, value_width)
    normed_heads = (
        hidden
        * lax.rsqrt(jnp.mean(hidden * hidden, axis=2, keepdims=True) + norm_floor)
        * head_gains
    )
    normed_heads = normed_heads.astype(jnp.bfloat16).reshape(group_len, local_heads * value_width)
    out_slab = lax.all_gather(w_out, "sp", axis=0, tiled=True)
    return lax.psum_scatter(
        lax.dot_general(
            normed_heads, out_slab, (((1,), (1,)), ((), ())), preferred_element_type=jnp.float32
        ).astype(jnp.bfloat16),
        "tp",
        scatter_dimension=0,
        tiled=True,
    )


ring_limit = 16
drift_span = 128
MESH = pl.DeviceIdType.MESH
f32 = jnp.float32
bf16 = jnp.bfloat16


def dot_nt(a, b):
    return lax.dot_general(a, b, (((1,), (1,)), ((), ())), preferred_element_type=f32)


def when(flag):
    return flag.astype(jnp.int32).astype(f32)


def square_kernel(
    n,
    tp,
    tokens,
    pre_gain,
    w_query,
    w_key,
    w_value,
    w_igate,
    w_fgate,
    forget_bias,
    drift,
    head_gain,
    w_out,
    out,
    tok_all,
    drift_in,
    normed,
    own_key,
    own_value,
    own_query,
    own_out,
    key_in,
    value_in,
    query_in,
    out_in,
    state_own,
    state_in,
    aux_own,
    aux_in,
    acc,
    heads,
    shares,
    pair_in,
    pair_sum,
    far_in,
    final_sum,
    shares_in,
    tok_send,
    tok_recv,
    drift_send,
    drift_recv,
    near_send,
    near_recv,
    far_send,
    far_recv,
    first_sems,
    first_recv,
    ring_send,
    ring_recv,
    state_send,
    state_recv,
    aux_send,
    aux_recv,
    pair_send,
    pair_recv,
    sum_send,
    sum_recv,
    share_send,
    share_recv,
):
    s = lax.axis_index("sp")
    t = lax.axis_index("tp")
    q = n // 2
    steps = q - 1
    zh = s // q
    r = s % q
    y = t // 2
    c = t % 2
    near = 2 * y + 1 - c
    head = 2 * (2 * y + zh) + c
    rows = tokens.shape[0]
    span_rows = rows * tp
    length = 2 * span_rows
    dk = w_query.shape[1] // 2
    dv = w_value.shape[1] // 2
    depth = w_query.shape[0]
    half = depth // 2
    half_ring = q // 2
    odd = r % 2
    pos = odd * (q - 1) + (1 - 2 * odd) * (r // 2)

    def owner_at(p):
        p = lax.rem(p + 2 * q, q)
        far = p // half_ring
        return far * (2 * (q - 1 - p) + 1) + (1 - far) * 2 * p

    targets = (zh * q + owner_at(pos + 1), zh * q + owner_at(pos - 1))

    barrier = pltpu.get_barrier_semaphore()
    me = s * tp + t
    for i in range(1, n * tp):
        other = lax.rem(me + i, n * tp)
        pl.semaphore_signal(
            barrier,
            inc=1,
            device_id={"sp": other // tp, "tp": lax.rem(other, tp)},
            device_id_type=MESH,
        )
    pl.semaphore_wait(barrier, n * tp - 1)

    copies = []
    guarded = []

    def remote(source, target, send, recv, sp_at, tp_at):
        return pltpu.make_async_remote_copy(
            src_ref=source,
            dst_ref=target,
            send_sem=send,
            recv_sem=recv,
            device_id={"sp": sp_at, "tp": tp_at},
            device_id_type=MESH,
        )

    def send(*args):
        copy = remote(*args)
        copy.start()
        copies.append(copy)
        return copy

    def send_or_keep(source, target, send_sem, recv_sem, sp_at, tp_at):
        away = (sp_at != s) | (tp_at != t)
        copy = remote(source, target, send_sem, recv_sem, sp_at, tp_at)

        @pl.when(away)
        def _():
            copy.start()

        @pl.when(jnp.logical_not(away))
        def _():
            pltpu.make_async_copy(source, target, recv_sem).start()

        guarded.append((away, copy))
        return copy

    def arrived(target, sem):
        pltpu.make_async_copy(target, target, sem).wait()

    pieces = (
        (0, w_key, own_key, key_in),
        (1, w_value, own_value, value_in),
        (2, w_query, own_query, query_in),
        (3, w_out, own_out, out_in),
    )
    stays = zh == c
    def first_send(p):
        _, own, stage, _ = pieces[p]
        width = own.shape[1] // 2
        for g in range(2):
            mine = own.at[:, pl.ds(g * width, width)]
            keep = stays & (c == g)
            block = (zh + c) % 2
            copy = remote(
                mine,
                stage.at[block],
                first_sems.at[g, p],
                first_recv.at[block, p],
                c * q + r,
                2 * y + g,
            )

            @pl.when(jnp.logical_not(keep))
            def _():
                copy.start()

            @pl.when(keep)
            def _():
                pltpu.make_async_copy(mine, stage.at[0], first_recv.at[0, p]).start()

            guarded.append((jnp.logical_not(keep), copy))

    for p in range(3):
        first_send(p)

    def ring_copy(p, block, d, k):
        _, _, stage, landing = pieces[p]
        size = stage.shape[1] // 2
        source = (
            stage.at[block, pl.ds(d * size, size)] if k == 0 else landing.at[block, d, k - 1]
        )
        return send(
            source,
            landing.at[block, d, k],
            ring_send.at[p, block, d, k],
            ring_recv.at[p, block, d, k],
            targets[d],
            t,
        )

    live = {}

    def ring_start(p, block):
        arrived(pieces[p][2].at[block], first_recv.at[block, p])
        for d in range(2):
            live[p, block, d] = ring_copy(p, block, d, 0)

    def ring_step(p, block, k):
        for d in range(2):
            live[p, block, d].wait_recv()
            if k + 1 < steps:
                live[p, block, d] = ring_copy(p, block, d, k + 1)

    cols = (slice(0, dk), slice(dk, dk + dv), slice(dk + dv, 2 * dk + dv))

    def origin(block, owner):
        return (zh if block == 0 else 1 - zh) * q + owner

    def own_product(block, fresh):
        at = pl.ds(pl.multiple_of(origin(block, r) * depth, depth), depth)
        part = normed[:, at]
        for p in range(3):
            product = jnp.dot(part, pieces[p][2][block], preferred_element_type=f32)
            acc[:, cols[p]] = product if fresh else acc[:, cols[p]] + product

    def step_product(block, k):
        for d in range(2):
            owner = owner_at(pos - 1 - k) if d == 0 else owner_at(pos + 1 + k)
            at = pl.ds(
                pl.multiple_of(origin(block, owner) * depth + d * half, half), half
            )
            part = normed[:, at]
            for p in range(3):
                acc[:, cols[p]] += jnp.dot(
                    part, pieces[p][3][block, d, k], preferred_element_type=f32
                )

    for p in range(3):
        ring_start(p, 0)
    half_tp = tp // 2
    x = s % 2
    row_at = pl.ds(pl.multiple_of(x * span_rows + t * rows, rows), rows)

    def tokens_at(xx, to_t):
        start = pl.multiple_of(xx * span_rows + to_t * rows, rows)
        return tok_all.at[pl.ds(start, rows)]

    for p in range(3):
        ring_step(p, 0, 0)
    for g in range(2):
        to_s = g * q + s // 2
        send_or_keep(
            tokens, tok_all.at[row_at], tok_send.at[g], tok_recv.at[x], to_s, t
        )
        send_or_keep(
            drift, drift_in.at[x], drift_send.at[g], drift_recv.at[x], to_s, t
        )
    for k in range(1, steps):
        for p in range(3):
            ring_step(p, 0, k)
    first_send(3)
    for p in range(3):
        ring_start(p, 1)
    for xx in range(2):
        block = tokens_at(xx, t)
        arrived(block, tok_recv.at[xx])
        arrived(drift_in.at[xx], drift_recv.at[xx])
        for i in range(1, half_tp):
            far_t = 2 * lax.rem(y + i, half_tp) + c
            send(block, block, far_send.at[xx, i - 1], far_recv.at[xx, i - 1], s, far_t)
        send(block, block, near_send.at[xx, 0], near_recv.at[xx, 0], s, near)
    for p in range(3):
        ring_step(p, 1, 0)
    for xx in range(2):
        for i in range(1, half_tp):
            block = tokens_at(xx, 2 * lax.rem(y - i + half_tp, half_tp) + c)
            arrived(block, far_recv.at[xx, i - 1])
            send(block, block, near_send.at[xx, i], near_recv.at[xx, i], s, near)
    for k in range(1, steps - 1):
        for p in range(3):
            ring_step(p, 1, k)
    ring_start(3, 0)
    for xx in range(2):
        for i in range(half_tp):
            block = tokens_at(xx, 2 * lax.rem(y - i + half_tp, half_tp) + 1 - c)
            arrived(block, near_recv.at[xx, i])
    wide = tok_all[...].astype(f32)
    scale = lax.rsqrt(jnp.mean(wide * wide, axis=1, keepdims=True) + norm_floor)
    normed[...] = (wide * scale * pre_gain[...].astype(f32)[None, :]).astype(bf16)

    own_product(0, True)
    for k in range(steps):
        step_product(0, k)
    own_product(1, False)
    for k in range(steps - 1):
        step_product(1, k)
    ring_step(3, 0, 0)
    all_normed = normed[...]
    gate_in = dot_nt(all_normed, w_igate[...])
    gate_forget = dot_nt(all_normed, w_fgate[...])
    row_id = lax.broadcasted_iota(jnp.int32, (length, length), 0)
    col_id = lax.broadcasted_iota(jnp.int32, (length, length), 1)
    causal = row_id >= col_id
    pick = lax.broadcasted_iota(jnp.int32, gate_in.shape, 1) == head
    late = lax.broadcasted_iota(jnp.int32, (length, 1), 0) >= span_rows
    mine = pl.ds(head, 1)
    offset = jnp.where(late, drift_in[1, mine, :][:, :1], drift_in[0, mine, :][:, :1])
    forget_pre = (
        jnp.sum(jnp.where(pick, gate_forget, 0.0), axis=1, keepdims=True)
        + forget_bias[head]
        + offset
    )
    lf_col = jnp.minimum(forget_pre, 0.0) - jnp.log1p(jnp.exp(-jnp.abs(forget_pre)))
    in_col = jnp.sum(jnp.where(pick, gate_in, 0.0), axis=1, keepdims=True)
    lf_row = jnp.sum(jnp.where(row_id == col_id, lf_col, 0.0), axis=0, keepdims=True)
    in_row = jnp.sum(jnp.where(row_id == col_id, in_col, 0.0), axis=0, keepdims=True)
    b_col = jnp.sum(jnp.where(causal, lf_row, 0.0), axis=1, keepdims=True)
    b_row = jnp.sum(jnp.where(row_id <= col_id, lf_col, 0.0), axis=0, keepdims=True)
    span = jnp.sum(lf_col, axis=0, keepdims=True)
    write = span - b_col + in_col
    top = jnp.max(write, axis=0, keepdims=True)
    write_scale = jnp.exp(write - top)
    log_pair = jnp.where(causal, b_col - b_row + in_row, lowest_log)
    peak = jnp.max(log_pair, axis=1, keepdims=True)
    decay = jnp.where(causal, jnp.exp(log_pair - peak), 0.0)

    for p in range(3):
        ring_step(p, 1, steps - 1)
    step_product(1, steps - 1)
    ring_start(3, 1)
    keys = (acc[:, cols[0]] * (dk**-0.5)).astype(bf16)
    values = acc[:, cols[1]].astype(bf16)
    queries = acc[:, cols[2]].astype(bf16)
    key_scaled = keys.astype(f32) * write_scale
    state_own[...] = jnp.dot(
        key_scaled.T.astype(bf16), values, preferred_element_type=f32
    ).astype(bf16)
    aux_own[0:1, :] = jnp.broadcast_to(span, (1, dk))
    aux_own[1:2, :] = jnp.broadcast_to(top, (1, dk))
    aux_own[2:3, :] = jnp.sum(key_scaled, axis=0, keepdims=True)
    aux_own[3:, :] = jnp.zeros((aux_own.shape[0] - 3, dk), f32)
    state_copies = []
    for i in range(1, q):
        peer = zh * q + lax.rem(r + i, q)
        state_copies.append(
            (
                send(
                    state_own,
                    state_in.at[i - 1],
                    state_send.at[i - 1],
                    state_recv.at[i - 1],
                    peer,
                    t,
                ),
                send(
                    aux_own,
                    aux_in.at[i - 1],
                    aux_send.at[i - 1],
                    aux_recv.at[i - 1],
                    peer,
                    t,
                ),
            )
        )
    weights = dot_nt(queries, keys) * decay
    numer = jnp.dot(weights.astype(bf16), values, preferred_element_type=f32)
    denom = jnp.sum(weights, axis=1, keepdims=True)
    ring_step(3, 0, 1)
    ring_step(3, 1, 0)
    for pair in state_copies:
        for copy in pair:
            copy.wait_recv()
    owners = [lax.rem(r - i + q, q) for i in range(1, q)]
    logs = []
    for k in range(steps):
        total = aux_in[k, 1:2, :]
        for i in range(steps):
            if i != k:
                between = when((owners[i] > owners[k]) & (owners[i] < r))
                total = total + between * aux_in[i, 0:1, :]
        before = when(owners[k] < r)
        logs.append((before, before * total + (1.0 - before) * lowest_log))
    entry = functools.reduce(jnp.maximum, [log for _, log in logs])
    mat = jnp.zeros((dk, dv), f32)
    vec = jnp.zeros((1, dk), f32)
    for k in range(steps):
        before, log = logs[k]
        weight = before * jnp.exp(log - entry)
        mat = mat + weight[:, :1] * state_in[k].astype(f32)
        vec = vec + weight * aux_in[k, 2:3, :]
    carried = b_col + entry[:, :1]
    new_top = jnp.maximum(peak, carried)
    w_intra = jnp.exp(peak - new_top)
    w_carry = jnp.exp(carried - new_top)
    numer = w_intra * numer + w_carry * jnp.dot(
        queries, mat.astype(bf16), preferred_element_type=f32
    )
    denom = w_intra * denom + w_carry * jnp.sum(
        queries.astype(f32) * vec, axis=1, keepdims=True
    )
    hidden = numer / jnp.maximum(jnp.abs(denom), jnp.exp(-new_top))
    gain = head_gain[pl.ds(pl.multiple_of(head * dv, dv), dv)].astype(f32)[None, :]
    heads[...] = (
        hidden
        * lax.rsqrt(jnp.mean(hidden * hidden, axis=1, keepdims=True) + norm_floor)
        * gain
    ).astype(bf16)

    ready = heads[...]
    e_depth = w_out.shape[0]
    e_half = e_depth // 2
    wide_half = q * e_depth
    theirs = pl.ds(pl.multiple_of((1 - c) * span_rows, span_rows), span_rows)
    kept = pl.ds(pl.multiple_of(c * span_rows, span_rows), span_rows)

    def share_own(block):
        at = pl.ds(pl.multiple_of(r * e_depth, e_depth), e_depth)
        shares[block, :, at] = dot_nt(ready, own_out[block]).astype(bf16)

    def share_step(block, k):
        for d in range(2):
            owner = owner_at(pos - 1 - k) if d == 0 else owner_at(pos + 1 + k)
            at = pl.ds(pl.multiple_of(owner * e_depth + d * e_half, e_half), e_half)
            shares[block, :, at] = dot_nt(ready, out_in[block, d, k]).astype(bf16)

    def pair_start(block):
        return send(
            shares.at[block, theirs],
            pair_in.at[block],
            pair_send.at[block],
            pair_recv.at[block],
            s,
            near,
        )

    def far_start(block, pair):
        pair.wait_recv()
        pair_sum[block] = (
            shares[block, kept, :].astype(f32) + pair_in[block].astype(f32)
        ).astype(bf16)
        found = []
        for i in range(1, half_tp):
            yy = lax.rem(y + i, half_tp)
            at = pl.ds(pl.multiple_of(yy * 2 * rows, 2 * rows), 2 * rows)
            found.append(
                send(
                    pair_sum.at[block, at],
                    far_in.at[block, i - 1],
                    sum_send.at[block, i - 1],
                    sum_recv.at[block, i - 1],
                    s,
                    2 * yy + c,
                )
            )
        return found

    def share_out(block, found):
        at = pl.ds(pl.multiple_of(y * 2 * rows, 2 * rows), 2 * rows)
        total = pair_sum[block, at, :].astype(f32)
        for i, copy in enumerate(found):
            copy.wait_recv()
            total = total + far_in[block, i].astype(f32)
        final_sum[block] = total.astype(bf16)
        side = zh if block == 0 else 1 - zh
        for cc in range(2):
            send_or_keep(
                final_sum.at[block, pl.ds(cc * rows, rows)],
                shares_in.at[zh, side],
                share_send.at[block, cc],
                share_recv.at[zh, side],
                2 * r + c,
                2 * y + cc,
            )

    share_own(0)
    for k in range(steps):
        if k > 1:
            ring_step(3, 0, k)
        share_step(0, k)
    pair = pair_start(0)
    share_own(1)
    for k in range(steps - 1):
        if k > 0:
            ring_step(3, 1, k)
        share_step(1, k)
    found = far_start(0, pair)
    ring_step(3, 1, steps - 1)
    share_step(1, steps - 1)
    pair = pair_start(1)
    share_out(0, found)
    found = far_start(1, pair)
    share_out(1, found)
    for side in range(2):
        total = jnp.zeros((rows, wide_half), f32)
        for g in range(2):
            arrived(shares_in.at[g, side], share_recv.at[g, side])
            total = total + shares_in[g, side].astype(f32)
        out[:, side * wide_half : (side + 1) * wide_half] = total.astype(bf16)
    for copy in copies:
        copy.wait_send()
    for away, copy in guarded:

        @pl.when(away)
        def _():
            copy.wait_send()


def on_device_ring(
    n,
    tp,
    tokens,
    pre_gain,
    w_query,
    w_key,
    w_value,
    w_igate,
    w_fgate,
    forget_bias,
    gate_drift,
    head_gain,
    w_out,
):
    heads = w_igate.shape[1]
    if heads != 2 * tp or gate_drift.shape[0] > drift_span:
        return on_device(
            tokens,
            pre_gain,
            w_query,
            w_key,
            w_value,
            w_igate,
            w_fgate,
            forget_bias,
            gate_drift,
            head_gain,
            w_out,
        )
    rows, width = tokens.shape
    length = 2 * rows * tp
    q = n // 2
    steps = q - 1
    half_tp = tp // 2
    dk = w_query.shape[1] // 2
    dv = w_value.shape[1] // 2
    features = w_out.shape[0] * n
    vmem = pl.BlockSpec(memory_space=pltpu.VMEM)
    dma = pltpu.SemaphoreType.DMA
    weights = (w_key, w_value, w_query, w_out)
    smem = pl.BlockSpec(memory_space=pltpu.SMEM)
    return pl.pallas_call(
        functools.partial(square_kernel, n, tp),
        out_shape=jax.ShapeDtypeStruct((rows, features), bf16),
        in_specs=[vmem] * 7 + [smem] + [vmem] * 3,
        out_specs=vmem,
        scratch_shapes=[
            pltpu.VMEM((length, width), bf16),
            pltpu.VMEM((2, heads, gate_drift.shape[0]), f32),
            pltpu.VMEM((length, width), bf16),
            *[pltpu.VMEM((2, w.shape[0], w.shape[1] // 2), bf16) for w in weights],
            *[
                pltpu.VMEM((2, 2, steps, w.shape[0] // 2, w.shape[1] // 2), bf16)
                for w in weights
            ],
            pltpu.VMEM((dk, dv), bf16),
            pltpu.VMEM((steps, dk, dv), bf16),
            pltpu.VMEM((8, dk), f32),
            pltpu.VMEM((steps, 8, dk), f32),
            pltpu.VMEM((length, 2 * dk + dv), f32),
            pltpu.VMEM((length, dv), bf16),
            pltpu.VMEM((2, length, features // 2), bf16),
            pltpu.VMEM((2, length // 2, features // 2), bf16),
            pltpu.VMEM((2, length // 2, features // 2), bf16),
            pltpu.VMEM((2, half_tp - 1, 2 * rows, features // 2), bf16),
            pltpu.VMEM((2, 2 * rows, features // 2), bf16),
            pltpu.VMEM((2, 2, rows, features // 2), bf16),
            dma((2,)),
            dma((2,)),
            dma((2,)),
            dma((2,)),
            dma((2, half_tp)),
            dma((2, half_tp)),
            dma((2, half_tp)),
            dma((2, half_tp)),
            dma((2, 4)),
            dma((2, 4)),
            dma((4, 2, 2, steps)),
            dma((4, 2, 2, steps)),
            dma((steps,)),
            dma((steps,)),
            dma((steps,)),
            dma((steps,)),
            dma((2,)),
            dma((2,)),
            dma((2, half_tp)),
            dma((2, half_tp)),
            dma((2, 2)),
            dma((2, 2)),
        ],
        compiler_params=pltpu.CompilerParams(collective_id=0, has_side_effects=True),
    )(
        tokens,
        pre_gain,
        w_query,
        w_key,
        w_value,
        w_igate.T,
        w_fgate.T,
        forget_bias,
        gate_drift.T,
        head_gain,
        w_out,
    )


def solution(mesh):
    in_specs = (
        P(("sp", "tp"), None),
        P(),
        P("sp", "tp"),
        P("sp", "tp"),
        P("sp", "tp"),
        P(),
        P(),
        P(),
        P("sp", None),
        P(),
        P("sp", "tp"),
    )
    out_specs = P(("sp", "tp"), None)
    body = on_device
    if mesh.shape["sp"] <= ring_limit and mesh.shape["sp"] % 4 == 0 and mesh.shape["tp"] % 4 == 0:
        body = functools.partial(on_device_ring, mesh.shape["sp"], mesh.shape["tp"])
    return jax.shard_map(
        body, mesh=mesh, in_specs=in_specs, out_specs=out_specs, check_vma=False
    )
```

profile of v0, /device:TPU:0, one launch (start us, length us, event | category | flops | bytes accessed | tf_op | source)
XLA Modules:
  0.0 72.8 jit_solution(16918521306720113220)
XLA Ops:
  0.0 71.3 %shard_map.109 = bf16[32,2048]{1,0:T(8,128)(2,1)} custom-call(bf16[32,2048]{1,0:T(8,128)(2,1)} %tokens.1, bf16[2048]{0:T(1024)(128)(2,1)} %pre_gain.1, bf16[256,256]{1,0:T(8,128)(2,1)} %w_query.1, bf16[256,256]{1,0:T(8,128)(2,1)} %w_key.1, bf16[256,512]{1,0:T(8,128)(2,1)} %w_value.1, bf16[8,2048]{1,0:T(8,128)(2,1)} %bitcast.3, bf16[8,2048]{1,0:T(8,128)(2,1)} %bitcast.4, ...), custom_call_target="tpu_custom_call" | custom-call | tf_op jit(solution)/shard_map/pallas_call | solution.py:779
  71.3 1.6 %copy.13 = bf16[32,2048]{1,0:T(8,128)(2,1)} copy(bf16[32,2048]{1,0:T(8,128)(2,1)} %shard_map.109) | data formatting | bytes 262144
where the time goes:
time: 73 us; the launch traced here: 72.8 us
  Pallas kernels  71.3 us (98%)
  local copies, waits for them, and re-layouts  1.57 us (2%)
    pallas_call x1, Pallas kernels, on_device_ring(): pl.pallas_call(functools.partial(square_kernel, n, tp), out_shape=jax.Sha...  71.3 us
    unnamed x1, local copies, waits for them, and re-layouts  1.57 us

commit v1 on v0

v1 whole, which is shorter than its diff:
```python
import functools

import jax
import jax.numpy as jnp
from jax import lax
from jax.experimental import pallas as pl
from jax.experimental.pallas import tpu as pltpu
from jax.sharding import PartitionSpec as P

BLOCK = 64


norm_floor = 0.1
lowest_log = -1e30
highest = lax.Precision.HIGHEST


def prefix(value, axis, combine, identity):
    peers, position = (lax.axis_size(axis), lax.axis_index(axis))
    everything = jax.tree.map(
        lambda part, kind: lax.all_gather(part.astype(kind), axis),
        value,
        jax.tree.map(lambda a: jnp.bfloat16 if a.dtype == jnp.float32 else a.dtype, value),
    )
    start = jax.tree.map(
        lambda part, zero: jnp.broadcast_to(jnp.asarray(zero, part.dtype), part.shape),
        value,
        identity,
    )

    def step(k, before):
        reached = k < position
        new = combine(
            before, jax.tree.map(lambda part, own: part[k].astype(own.dtype), everything, value)
        )
        return jax.tree.map(lambda a, b: jnp.where(reached, a, b), new, before)

    return lax.fori_loop(0, peers, step, start)


def advance(memory, summary):
    old_mat, old_vec, old_top = memory
    span_log, span_top, span_mat, span_vec = summary
    new_top = jnp.maximum(span_log + old_top, span_top)
    kept_part = jnp.exp(span_log + old_top - new_top)
    fresh_part = jnp.exp(span_top - new_top)
    return (
        kept_part[:, None, None] * old_mat + fresh_part[:, None, None] * span_mat,
        kept_part[:, None] * old_vec + fresh_part[:, None] * span_vec,
        new_top,
    )


def prefix_states(initial, summary):

    def stepper(memory, one_block):
        return (advance(memory, one_block), memory)

    return lax.scan(stepper, initial, summary)


def join_devices(earlier, later_part):
    early_log, early_mat, early_vec, early_top = earlier
    late_log, late_mat, late_vec, late_top = later_part
    new_top = jnp.maximum(late_log + early_top, late_top)
    kept_part = jnp.exp(late_log + early_top - new_top)
    fresh_part = jnp.exp(late_top - new_top)
    return (
        early_log + late_log,
        kept_part[:, None, None] * early_mat + fresh_part[:, None, None] * late_mat,
        kept_part[:, None] * early_vec + fresh_part[:, None] * late_vec,
        new_top,
    )


def blend_parts(first_part, second_part):
    numer_first, denom_first, peak_first = first_part
    numer_second, denom_second, peak_second = second_part
    new_top = jnp.maximum(peak_first, peak_second)
    weight_first = jnp.exp(peak_first - new_top)
    weight_second = jnp.exp(peak_second - new_top)
    return (
        weight_first[..., None] * numer_first + weight_second[..., None] * numer_second,
        weight_first * denom_first + weight_second * denom_second,
        new_top,
    )


def on_device(
    tokens,
    pre_gain,
    w_query,
    w_key,
    w_value,
    w_igate,
    w_fgate,
    forget_bias,
    gate_drift,
    head_gain,
    w_out,
):
    tp_size = lax.axis_size("tp")
    head_count = w_igate.shape[1]
    local_heads = head_count // tp_size
    first_head = lax.axis_index("tp") * local_heads
    key_width = w_query.shape[1] // local_heads
    value_width = w_value.shape[1] // local_heads
    token_wide = tokens.astype(jnp.float32)
    scaled = token_wide * lax.rsqrt(
        jnp.mean(token_wide * token_wide, axis=1, keepdims=True) + norm_floor
    )
    normed = (scaled * pre_gain.astype(jnp.float32)).astype(jnp.bfloat16)
    gate_cols = jnp.concatenate(
        [
            lax.dynamic_slice_in_dim(w_igate, first_head, local_heads, 1),
            lax.dynamic_slice_in_dim(w_fgate, first_head, local_heads, 1),
        ],
        axis=1,
    )
    key_scale = key_width ** (-0.5)
    wq_full, wk_full, wv_full = (
        lax.all_gather(w_query, "sp", axis=0, tiled=True),
        lax.all_gather(w_key, "sp", axis=0, tiled=True),
        lax.all_gather(w_value, "sp", axis=0, tiled=True),
    )
    row_piece = lax.all_gather(normed, "tp", axis=0, tiled=True)
    queries_part = jnp.dot(row_piece, wq_full, preferred_element_type=jnp.float32).astype(
        jnp.bfloat16
    )
    keys_part = (
        jnp.dot(row_piece, wk_full, preferred_element_type=jnp.float32) * key_scale
    ).astype(jnp.bfloat16)
    values_part = jnp.dot(row_piece, wv_full, preferred_element_type=jnp.float32).astype(
        jnp.bfloat16
    )
    gate_part = jnp.dot(row_piece, gate_cols, preferred_element_type=jnp.float32)
    group_len = queries_part.shape[0]
    blocks = group_len // BLOCK
    log_input = gate_part[:, :local_heads]
    forget_pre = gate_part[:, local_heads:] + lax.dynamic_slice_in_dim(
        forget_bias, first_head, local_heads, 0
    )
    log_forget = jax.nn.log_sigmoid(
        forget_pre + lax.dynamic_slice_in_dim(gate_drift, first_head, local_heads, 1)
    )
    query_blk = queries_part.reshape(blocks, BLOCK, local_heads, key_width)
    key_blk = keys_part.reshape(blocks, BLOCK, local_heads, key_width)
    value_blk = values_part.reshape(blocks, BLOCK, local_heads, value_width)
    input_blk = log_input.reshape(blocks, BLOCK, local_heads).transpose(0, 2, 1)
    forget_blk = log_forget.reshape(blocks, BLOCK, local_heads).transpose(0, 2, 1)
    within = jnp.cumsum(forget_blk, axis=2)
    causal = jnp.arange(BLOCK)[:, None] >= jnp.arange(BLOCK)[None, :]
    log_pair = jnp.where(
        causal, within[..., :, None] - within[..., None, :] + input_blk[..., None, :], -jnp.inf
    )
    peak_intra = jnp.max(log_pair, axis=3)
    scores = jnp.einsum("nshd,nrhd->nhsr", query_blk, key_blk, preferred_element_type=jnp.float32)
    weights = scores * jnp.exp(log_pair - peak_intra[..., None])
    numer_intra = jnp.einsum(
        "nhsr,nrhv->nhsv",
        weights.astype(jnp.bfloat16),
        value_blk,
        preferred_element_type=jnp.float32,
    )
    denom_intra = jnp.sum(weights, axis=3)
    span_log = within[..., -1]
    log_write = span_log[..., None] - within + input_blk
    span_top = jnp.max(log_write, axis=2)
    write_scale = jnp.exp(log_write - span_top[..., None])
    key_scaled = key_blk.astype(jnp.float32) * write_scale.transpose(0, 2, 1)[..., None]
    value_wide = value_blk.astype(jnp.float32)
    span_mat = jnp.einsum("nrhv,nrhd->nhvd", value_wide, key_scaled, precision=highest)
    span_vec = jnp.sum(key_scaled, axis=1)
    summary = (span_log, span_top, span_mat, span_vec)
    empty_state = (
        jnp.zeros((local_heads, value_width, key_width), jnp.float32),
        jnp.zeros((local_heads, key_width), jnp.float32),
        jnp.full((local_heads,), lowest_log, jnp.float32),
    )
    local_end, local_starts = prefix_states(empty_state, summary)
    device_summary = (jnp.sum(span_log, axis=0),) + local_end
    identity_all = (jnp.zeros((local_heads,), jnp.float32),) + empty_state
    incoming = prefix(device_summary, "sp", join_devices, identity_all)
    query_wide = query_blk.astype(jnp.float32)
    intra_part = (numer_intra, denom_intra, peak_intra)
    start_mat, start_vec, start_top = local_starts
    local_part = (
        jnp.einsum("nhvd,nshd->nhsv", start_mat, query_wide, precision=highest),
        jnp.einsum("nhd,nshd->nhs", start_vec, query_wide, precision=highest),
        within + start_top[..., None],
    )
    numerator, denominator, peak_log = blend_parts(local_part, intra_part)
    entry_log, entry_mat, entry_vec, entry_top = incoming
    before_log = jnp.concatenate(
        [jnp.zeros((1, local_heads), jnp.float32), jnp.cumsum(span_log, axis=0)[:-1]], axis=0
    )
    from_left = (
        jnp.einsum("hvd,nshd->nhsv", entry_mat, query_wide, precision=highest),
        jnp.einsum("hd,nshd->nhs", entry_vec, query_wide, precision=highest),
        within + (before_log + entry_top[None, :])[..., None],
    )
    numerator, denominator, peak_log = blend_parts((numerator, denominator, peak_log), from_left)
    hidden = numerator / jnp.maximum(jnp.abs(denominator), jnp.exp(-peak_log))[..., None]
    hidden = hidden.transpose(0, 2, 1, 3).reshape(group_len, local_heads, value_width)
    head_gains = lax.dynamic_slice_in_dim(
        head_gain, first_head * value_width, local_heads * value_width, 0
    )
    head_gains = head_gains.astype(jnp.float32).reshape(local_heads, value_width)
    normed_heads = (
        hidden
        * lax.rsqrt(jnp.mean(hidden * hidden, axis=2, keepdims=True) + norm_floor)
        * head_gains
    )
    normed_heads = normed_heads.astype(jnp.bfloat16).reshape(group_len, local_heads * value_width)
    out_slab = lax.all_gather(w_out, "sp", axis=0, tiled=True)
    return lax.psum_scatter(
        lax.dot_general(
            normed_heads, out_slab, (((1,), (1,)), ((), ())), preferred_element_type=jnp.float32
        ).astype(jnp.bfloat16),
        "tp",
        scatter_dimension=0,
        tiled=True,
    )


drift_span = 128
MESH = pl.DeviceIdType.MESH
f32 = jnp.float32
bf16 = jnp.bfloat16


def dot_nt(a, b):
    return lax.dot_general(a, b, (((1,), (1,)), ((), ())), preferred_element_type=f32)


def layer_kernel(
    n,
    tp,
    tokens,
    pre_gain,
    w_key,
    w_value,
    w_query,
    w_igate,
    w_fgate,
    forget_bias,
    drift,
    head_gain,
    w_out,
    out,
    tok_own,
    tok_all,
    normed,
    gain_in,
    igate_in,
    fgate_in,
    bias_in,
    head_gain_in,
    drift_in,
    key_own,
    value_own,
    query_own,
    key_all,
    value_all,
    query_all,
    out_all,
    acc,
    state_all,
    aux_all,
    heads,
    heads_in,
    part,
    final_in,
    load_sems,
    tok_send,
    tok_recv,
    drift_send,
    drift_recv,
    w_send,
    w_recv,
    out_send,
    out_recv,
    state_send,
    state_recv,
    aux_send,
    aux_recv,
    heads_send,
    heads_recv,
    final_send,
    final_recv,
):
    s = lax.axis_index("sp")
    t = lax.axis_index("tp")
    layers = n // 2
    z = s // 2
    x = s % 2
    y = t // 2
    c = t % 2
    zh = z // 2
    zl = z % 2
    near = zh == c
    far = jnp.logical_not(near)
    head = layers * y + z
    rows = tok_own.shape[0]
    span = rows * tp
    length = 2 * span
    depth = key_own.shape[1]
    dk = key_own.shape[2]
    dv = value_own.shape[2]

    def flip(value):
        return 1 - value

    def at_layer(dz):
        if dz == 0:
            return z
        if dz == 1:
            return 2 * zh + flip(zl)
        if dz == 2:
            return 2 * flip(zh) + zl
        return 2 * flip(zh) + flip(zl)

    def dev(zz, xx, yy, cc):
        return 2 * zz + xx, 2 * yy + cc

    def load(source, target, sem):
        copy = pltpu.make_async_copy(source, target, sem)
        copy.start()
        return copy

    pieces = (
        (w_key, key_own, key_all),
        (w_value, value_own, value_all),
        (w_query, query_own, query_all),
    )

    def token_slot(parity, to_t):
        start = pl.multiple_of((parity * tp + to_t) * rows, rows)
        return tok_all.at[pl.ds(start, rows)]

    own_slot = token_slot(zl, t)
    load_tokens = load(tokens, tok_own, load_sems.at[0])
    loads_own = []
    for p, (w_hbm, own, full) in enumerate(pieces):
        width = own.shape[2]
        loads_own.append(
            [
                load(
                    w_hbm.at[:, pl.ds(j * width, width)],
                    own.at[j],
                    load_sems.at[1 + 2 * p + j],
                )
                for j in range(2)
            ]
        )
    chunk = out_all.shape[3] // 2
    loads_out = [
        load(
            w_out.at[pl.ds(i * chunk, chunk)],
            out_all.at[zh, x, c, pl.ds(i * chunk, chunk)],
            load_sems.at[7 + i],
        )
        for i in range(2)
    ]
    small = (
        (pre_gain, gain_in),
        (w_igate, igate_in),
        (w_fgate, fgate_in),
        (forget_bias, bias_in),
        (head_gain, head_gain_in),
    )
    loads_small = [load(a, b, load_sems.at[9 + i]) for i, (a, b) in enumerate(small)]

    @pl.when(near)
    def _():
        pltpu.make_async_copy(tokens, own_slot, tok_recv.at[zl, 0, c]).start()
        pltpu.make_async_copy(drift, drift_in.at[zl], drift_recv.at[zl]).start()
        for p, (w_hbm, own, full) in enumerate(pieces):
            width = own.shape[2]
            for j in range(2):

                @pl.when(zl == j)
                def _():
                    pltpu.make_async_copy(
                        w_hbm.at[:, pl.ds(j * width, width)], full.at[s], w_recv.at[p, s]
                    ).start()

    load_drift = load(drift, drift_in.at[2], load_sems.at[14])

    barrier = pltpu.get_barrier_semaphore()
    me = s * tp + t
    for i in range(1, n * tp):
        other = lax.rem(me + i, n * tp)
        pl.semaphore_signal(
            barrier,
            inc=1,
            device_id={"sp": other // tp, "tp": lax.rem(other, tp)},
            device_id_type=MESH,
        )

    @pl.when(c == 0)
    def _():
        state_all[layers:, :, :] = jnp.zeros((layers, dk, dv), bf16)
        aux_all[layers:, :, :] = jnp.zeros((layers, aux_all.shape[1], dk), f32)

    pl.semaphore_wait(barrier, n * tp - 1)

    started = []

    def send(source, target, send_sem, recv_sem, to, flag=None, keep=None):
        copy = pltpu.make_async_remote_copy(
            src_ref=source,
            dst_ref=target,
            send_sem=send_sem,
            recv_sem=recv_sem,
            device_id={"sp": to[0], "tp": to[1]},
            device_id_type=MESH,
        )
        if keep is not None:

            @pl.when(keep)
            def _():
                pltpu.make_async_copy(source, target, recv_sem).start()

            flag = jnp.logical_not(keep)
        if flag is None:
            copy.start()
        else:

            @pl.when(flag)
            def _():
                copy.start()

        started.append((flag, copy))

    def arrived(target, sem):
        pltpu.make_async_copy(target, target, sem).wait()

    load_tokens.wait()
    mine = tok_recv.at[zl, 0, c]
    send(tok_own, own_slot, tok_send.at[0], mine, dev(at_layer(2), x, y, zh))
    send(tok_own, own_slot, tok_send.at[1], mine, dev(at_layer(1), x, y, zh))
    send(
        tok_own, own_slot, tok_send.at[2], tok_recv.at[zl, 1, c], dev(z, x, flip(y), zh)
    )
    send(tok_own, own_slot, tok_send.at[3], mine, dev(z, x, y, flip(c)), flag=far)
    load_drift.wait()
    for i in range(1, 4):
        send(
            drift_in.at[2],
            drift_in.at[zl],
            drift_send.at[i - 1],
            drift_recv.at[zl],
            dev(at_layer(i), x, y, c),
            flag=near,
        )

    layer_a = 2 * c + zl
    layer_b = 2 * c + flip(zl)

    def first_send(p):
        _, own, full = pieces[p]
        for j in range(2):
            loads_own[p][j].wait()
        send(
            own.at[zl],
            full.at[s],
            w_send.at[p, 0],
            w_recv.at[p, s],
            dev(layer_a, x, y, zh),
            flag=far,
        )
        send(
            own.at[flip(zl)],
            full.at[s],
            w_send.at[p, 1],
            w_recv.at[p, s],
            dev(layer_b, x, y, zh),
        )

    def pass_on(p, block, i, across):
        _, _, full = pieces[p]
        sem = w_recv.at[p, block]
        arrived(full.at[block], sem)
        if across:
            send(full.at[block], full.at[block], w_send.at[p, 2 + i], sem, dev(z, flip(x), y, c))
        send(full.at[block], full.at[block], w_send.at[p, 4 + i], sem, dev(z, x, y, flip(c)))

    block_a = 2 * layer_a + x
    block_b = 2 * layer_b + x
    cross_a = 2 * layer_a + flip(x)
    cross_b = 2 * layer_b + flip(x)

    def pass_first(p, which):
        pass_on(p, (block_a, block_b)[which], which, True)

    def pass_cross(p):
        pass_on(p, cross_a, 2, False)
        pass_on(p, cross_b, 3, False)

    for p in range(3):
        first_send(p)

    def out_chunk(zb, xb, cb, i):
        return out_all.at[zb, xb, cb, pl.ds(i * chunk, chunk)]

    def out_pass(zb, xb, i, base, to):
        for k, target in enumerate(to):
            part_ref = out_chunk(zb, xb, c, i)
            send(
                part_ref,
                part_ref,
                out_send.at[base + k, i],
                out_recv.at[zb, xb, c, i],
                target,
            )

    to_x = dev(z, flip(x), y, c)
    to_core = dev(z, x, y, flip(c))
    to_half = dev(at_layer(2), x, y, c)

    def token_pass(parity, c_src, i, onward):
        slot = token_slot(parity, 2 * y + c_src)
        arrived(slot, tok_recv.at[parity, 0, c_src])
        if onward:
            send(
                slot,
                slot,
                tok_send.at[4 + i],
                tok_recv.at[parity, 0, c_src],
                dev(at_layer(1), x, y, c),
                flag=far,
            )
        send(
            slot,
            slot,
            tok_send.at[6 + i],
            tok_recv.at[parity, 1, c_src],
            dev(z, x, flip(y), c),
            flag=far if onward else None,
        )

    for copy in loads_small:
        copy.wait()
    gain = gain_in[...].astype(f32)

    def normalize(parity, to_t):
        start = pl.multiple_of((parity * tp + to_t) * rows, rows)
        wide = tok_all[pl.ds(start, rows), :].astype(f32)
        scale = lax.rsqrt(jnp.mean(wide * wide, axis=1, keepdims=True) + norm_floor)
        normed[pl.ds(start, rows), :] = (wide * scale * gain).astype(bf16)

    for c_src in range(2):
        token_pass(zl, c_src, c_src, True)
    for c_src in range(2):
        token_pass(flip(zl), c_src, 2 + c_src, False)
    for copy in loads_out:
        copy.wait()
    for i in range(2):
        out_pass(zh, x, i, 0, (to_x, to_core))
    pass_first(0, 0)
    pass_first(0, 1)
    for parity in range(2):
        for c_src in range(2):
            normalize(parity, 2 * y + c_src)
    pass_cross(0)
    pass_first(1, 0)
    pass_first(1, 1)
    for parity in range(2):
        for c_src in range(2):
            to_t = 2 * flip(y) + c_src
            arrived(token_slot(parity, to_t), tok_recv.at[parity, 1, c_src])
            normalize(parity, to_t)

    cols = (slice(0, dk), slice(dk, dk + dv), slice(dk + dv, 2 * dk + dv))
    direct = (block_a, block_b, cross_a, cross_b)
    relayed = [2 * (2 * flip(c) + k) + xx for k in range(2) for xx in range(2)]

    def product(p, block, fresh):
        at = pl.ds(pl.multiple_of(block * depth, depth), depth)
        term = jnp.dot(normed[:, at], pieces[p][2][block], preferred_element_type=f32)
        acc[:, cols[p]] = term if fresh else acc[:, cols[p]] + term

    def direct_products(p):
        for i, block in enumerate(direct):
            product(p, block, i == 0)

    def relayed_products(p):
        for block in relayed:
            arrived(pieces[p][2].at[block], w_recv.at[p, block])
            product(p, block, False)

    direct_products(0)
    pass_cross(1)
    for i in range(2):
        out_pass(zh, x, i, 2, (to_half,))
    relayed_products(0)

    all_normed = normed[...]
    gate_in = dot_nt(all_normed, igate_in[...])
    gate_forget = dot_nt(all_normed, fgate_in[...])
    pick = lax.broadcasted_iota(jnp.int32, gate_in.shape, 1) == head
    pick_bias = lax.broadcasted_iota(jnp.int32, bias_in.shape, 1) == head
    bias = jnp.sum(jnp.where(pick_bias, bias_in[...], 0.0), axis=1, keepdims=True)
    forget_all = jnp.sum(jnp.where(pick, gate_forget, 0.0), axis=1, keepdims=True) + bias
    input_all = jnp.sum(jnp.where(pick, gate_in, 0.0), axis=1, keepdims=True)
    row_id = lax.broadcasted_iota(jnp.int32, (span, span), 0)
    col_id = lax.broadcasted_iota(jnp.int32, (span, span), 1)
    causal = row_id >= col_id
    eye = row_id == col_id
    gates = []
    for j in range(2):
        arrived(drift_in.at[j], drift_recv.at[j])
        offset = drift_in[j, pl.ds(head, 1), :][:, :1]
        pre = forget_all[j * span : (j + 1) * span] + offset
        in_col = input_all[j * span : (j + 1) * span]
        lf_col = jnp.minimum(pre, 0.0) - jnp.log1p(jnp.exp(-jnp.abs(pre)))
        lf_row = jnp.sum(jnp.where(eye, lf_col, 0.0), axis=0, keepdims=True)
        in_row = jnp.sum(jnp.where(eye, in_col, 0.0), axis=0, keepdims=True)
        b_col = jnp.sum(jnp.where(causal, lf_row, 0.0), axis=1, keepdims=True)
        b_row = jnp.sum(jnp.where(row_id <= col_id, lf_col, 0.0), axis=0, keepdims=True)
        total = jnp.sum(lf_col, axis=0, keepdims=True)
        write = total - b_col + in_col
        top = jnp.max(write, axis=0, keepdims=True)
        write_scale = jnp.exp(write - top)
        log_pair = jnp.where(causal, b_col - b_row + in_row, lowest_log)
        peak = jnp.max(log_pair, axis=1, keepdims=True)
        decay = jnp.where(causal, jnp.exp(log_pair - peak), 0.0)
        gates.append((b_col, total, top, write_scale, peak, decay))

    pass_first(2, 0)
    pass_first(2, 1)
    direct_products(1)
    relayed_products(1)
    pass_cross(2)

    spans = [4 * c + 2 * j + x for j in range(2)]
    keys = (acc[:, cols[0]] * (dk**-0.5)).astype(bf16)
    values = acc[:, cols[1]].astype(bf16)
    for j in range(2):
        b_col, total, top, write_scale, peak, decay = gates[j]
        at = slice(j * span, (j + 1) * span)
        key_scaled = keys[at].astype(f32) * write_scale
        state_all[spans[j]] = jnp.dot(
            key_scaled.T.astype(bf16), values[at], preferred_element_type=f32
        ).astype(bf16)
        mine = spans[j]
        aux_all[mine, 0:1, :] = jnp.broadcast_to(total, (1, dk))
        aux_all[mine, 1:2, :] = jnp.broadcast_to(top, (1, dk))
        aux_all[mine, 2:3, :] = jnp.sum(key_scaled, axis=0, keepdims=True)
        aux_all[mine, 3:, :] = jnp.zeros((aux_all.shape[1] - 3, dk), f32)
    late = c == 1
    early = c == 0
    for k, (to, flag) in enumerate(
        (
            (dev(z, flip(x), y, c), None),
            (dev(z, flip(x), y, flip(c)), early),
            (dev(z, x, y, flip(c)), early),
        )
    ):
        for j in range(2):
            mine = spans[j]
            send(
                aux_all.at[mine],
                aux_all.at[mine],
                aux_send.at[k, j],
                aux_recv.at[mine],
                to,
                flag=flag,
            )
            send(
                state_all.at[mine],
                state_all.at[mine],
                state_send.at[k, j],
                state_recv.at[mine],
                to,
                flag=flag,
            )

    direct_products(2)
    relayed_products(2)
    queries = acc[:, cols[2]].astype(bf16)
    intra = []
    for j in range(2):
        b_col, total, top, write_scale, peak, decay = gates[j]
        at = slice(j * span, (j + 1) * span)
        weights = dot_nt(queries[at], keys[at]) * decay
        numer = jnp.dot(weights.astype(bf16), values[at], preferred_element_type=f32)
        denom = jnp.sum(weights, axis=1, keepdims=True)
        intra.append((numer, denom))

    for j in range(2):
        theirs = 4 * c + 2 * j + flip(x)
        arrived(aux_all.at[theirs], aux_recv.at[theirs])
        arrived(state_all.at[theirs], state_recv.at[theirs])

    @pl.when(late)
    def _():
        for m in range(layers):
            arrived(aux_all.at[m], aux_recv.at[m])
            arrived(state_all.at[m], state_recv.at[m])

    span_rows = aux_all[:, 0, :]
    top_rows = aux_all[:, 1, :]
    vec_rows = aux_all[:, 2, :]
    place = lax.broadcasted_iota(jnp.int32, span_rows.shape, 0)
    gain_row = head_gain_in[:, pl.ds(pl.multiple_of(head * dv, dv), dv)].astype(f32)
    for j in range(2):
        b_col, total, top, write_scale, peak, decay = gates[j]
        numer, denom = intra[j]
        at = slice(j * span, (j + 1) * span)
        before = place < spans[j]
        logs = top_rows
        for m in range(1, n):
            between = (place < m) & (spans[j] > m)
            logs = logs + jnp.where(between, span_rows[m : m + 1, :], 0.0)
        logs = jnp.where(before, logs, lowest_log)
        entry = jnp.max(logs, axis=0, keepdims=True)
        weight = jnp.where(before, jnp.exp(logs - entry), 0.0)
        vec = jnp.sum(weight * vec_rows, axis=0, keepdims=True)
        mat = jnp.zeros((dk, dv), f32)
        for m in range(n - 1):
            mat = mat + weight[m : m + 1, :1] * state_all[m].astype(f32)
        carried = b_col + entry[:, :1]
        new_top = jnp.maximum(peak, carried)
        w_intra = jnp.exp(peak - new_top)
        w_carry = jnp.exp(carried - new_top)
        numer = w_intra * numer + w_carry * jnp.dot(
            queries[at], mat.astype(bf16), preferred_element_type=f32
        )
        denom = w_intra * denom + w_carry * jnp.sum(
            queries[at].astype(f32) * vec, axis=1, keepdims=True
        )
        hidden = numer / jnp.maximum(jnp.abs(denom), jnp.exp(-new_top))
        heads[j] = (
            hidden
            * lax.rsqrt(jnp.mean(hidden * hidden, axis=1, keepdims=True) + norm_floor)
            * gain_row
        ).astype(bf16)
        for d in range(2):
            send(
                heads.at[j],
                heads_in.at[z],
                heads_send.at[j, d],
                heads_recv.at[z],
                dev(2 * c + d, x, y, j),
                keep=near & (zl == d) & (c == j),
            )

    for i in range(2):
        arrived(out_chunk(zh, flip(x), c, i), out_recv.at[zh, flip(x), c, i])
        out_pass(zh, flip(x), i, 3, (to_core,))
    for i in range(2):
        arrived(out_chunk(flip(zh), x, c, i), out_recv.at[flip(zh), x, c, i])
        out_pass(flip(zh), x, i, 4, (to_x, to_core))
    for i in range(2):
        arrived(out_chunk(flip(zh), flip(x), c, i), out_recv.at[flip(zh), flip(x), c, i])
        out_pass(flip(zh), flip(x), i, 6, (to_core,))
    for zb in range(2):
        for xb in range(2):
            for i in range(2):
                arrived(out_chunk(zb, xb, flip(c), i), out_recv.at[zb, xb, flip(c), i])
    for m in range(layers):
        arrived(heads_in.at[m], heads_recv.at[m])

    features = out_all.shape[3]
    home = 2 * zh + c
    for zb in range(2):
        for xb in range(2):
            total = jnp.zeros((span, features), f32)
            for m in range(layers):
                total = total + dot_nt(
                    heads_in[m], out_all[zb, xb, m // 2, :, (m % 2) * dv : (m % 2 + 1) * dv]
                )
            part[zb, :, xb * features : (xb + 1) * features] = total.astype(bf16)
        for yy in range(2):
            for cc in range(2):
                send(
                    part.at[zb, pl.ds((2 * yy + cc) * rows, rows)],
                    final_in.at[zl, y, zb],
                    final_send.at[zb, yy, cc],
                    final_recv.at[zl, y, zb],
                    dev(home, x, yy, cc),
                    keep=(zl == c) & (y == yy) & (c == cc),
                )
    wide = 2 * features
    for zb in range(2):
        for zz in range(2):
            total = jnp.zeros((rows, wide), f32)
            for yy in range(2):
                arrived(final_in.at[zz, yy, zb], final_recv.at[zz, yy, zb])
                total = total + final_in[zz, yy, zb].astype(f32)
            at = (zz + 2 * zb) * wide
            out[:, at : at + wide] = total.astype(bf16)

    for flag, copy in started:
        if flag is None:
            copy.wait_send()
        else:

            @pl.when(flag)
            def _():
                copy.wait_send()


def on_device_layers(
    n,
    tp,
    tokens,
    pre_gain,
    w_query,
    w_key,
    w_value,
    w_igate,
    w_fgate,
    forget_bias,
    gate_drift,
    head_gain,
    w_out,
):
    heads = w_igate.shape[1]
    rows, width = tokens.shape
    span = rows * tp
    if (
        heads != 2 * tp
        or n != heads
        or gate_drift.shape[0] != span
        or span > drift_span
    ):
        return on_device(
            tokens,
            pre_gain,
            w_query,
            w_key,
            w_value,
            w_igate,
            w_fgate,
            forget_bias,
            gate_drift,
            head_gain,
            w_out,
        )
    layers = n // 2
    depth = w_query.shape[0]
    dk = w_query.shape[1] // 2
    dv = w_value.shape[1] // 2
    features = w_out.shape[0]
    anywhere = pl.BlockSpec(memory_space=pl.ANY)
    dma = pltpu.SemaphoreType.DMA
    vmem = pltpu.VMEM
    return pl.pallas_call(
        functools.partial(layer_kernel, n, tp),
        out_shape=jax.ShapeDtypeStruct((rows, features * n), bf16),
        in_specs=[anywhere] * 11,
        out_specs=pl.BlockSpec(memory_space=pltpu.VMEM),
        scratch_shapes=[
            vmem((rows, width), bf16),
            vmem((2 * span, width), bf16),
            vmem((2 * span, width), bf16),
            vmem((1, width), bf16),
            vmem((heads, width), bf16),
            vmem((heads, width), bf16),
            vmem((1, heads), f32),
            vmem((1, heads * dv), bf16),
            vmem((3, heads, span), f32),
            vmem((2, depth, dk), bf16),
            vmem((2, depth, dv), bf16),
            vmem((2, depth, dk), bf16),
            vmem((n, depth, dk), bf16),
            vmem((n, depth, dv), bf16),
            vmem((n, depth, dk), bf16),
            vmem((2, 2, 2, features, 2 * dv), bf16),
            vmem((2 * span, 2 * dk + dv), f32),
            vmem((n, dk, dv), bf16),
            vmem((n, 8, dk), f32),
            vmem((2, span, dv), bf16),
            vmem((layers, span, dv), bf16),
            vmem((2, span, 2 * features), bf16),
            vmem((2, 2, 2, rows, 2 * features), bf16),
            dma((15,)),
            dma((10,)),
            dma((2, 2, 2)),
            dma((3,)),
            dma((2,)),
            dma((3, 8)),
            dma((3, n)),
            dma((7, 2)),
            dma((2, 2, 2, 2)),
            dma((3, 2)),
            dma((n,)),
            dma((3, 2)),
            dma((n,)),
            dma((2, 2)),
            dma((layers,)),
            dma((2, 2, 2)),
            dma((2, 2, 2)),
        ],
        compiler_params=pltpu.CompilerParams(collective_id=0, has_side_effects=True),
    )(
        tokens,
        pre_gain[None, :],
        w_key,
        w_value,
        w_query,
        w_igate.T,
        w_fgate.T,
        forget_bias[None, :],
        gate_drift.T,
        head_gain[None, :],
        w_out,
    )


def solution(mesh):
    in_specs = (
        P(("sp", "tp"), None),
        P(),
        P("sp", "tp"),
        P("sp", "tp"),
        P("sp", "tp"),
        P(),
        P(),
        P(),
        P("sp", None),
        P(),
        P("sp", "tp"),
    )
    out_specs = P(("sp", "tp"), None)
    body = on_device
    if mesh.shape["sp"] == 2 * mesh.shape["tp"] and mesh.shape["tp"] == 4:
        body = functools.partial(on_device_layers, mesh.shape["sp"], mesh.shape["tp"])
    return jax.shard_map(
        body, mesh=mesh, in_specs=in_specs, out_specs=out_specs, check_vma=False
    )
```

time: 73 us -> 67.2 us (0.921); the launches traced: 72.8 us -> 65.9 us
  Pallas kernels: 71.3 us -> 62.3 us
  local copies, waits for them, and re-layouts: 1.57 us -> 3.55 us
    pallas_call x1, Pallas kernels: 71.3 us -> 62.3 us  [on_device_layers(): pl.pallas_call(functools.partial(layer_kernel, n, tp), out_shape=jax.Shap...]
    broadcast_in_dim x0 -> x2, local copies, waits for them, and re-layouts: none -> 1.21 us  [the longest x1 0.6 us: on_device_layers(): pre_gain[None, :]]
    unnamed x1 -> x5, local copies, waits for them, and re-layouts: 1.57 us -> 2.34 us
where the time goes in v1:
time: 67.2 us; the launch traced here: 65.9 us
  Pallas kernels  62.3 us (93%)
  local copies, waits for them, and re-layouts  3.55 us (5%)
    pallas_call x1, Pallas kernels, on_device_layers(): pl.pallas_call(functools.partial(layer_kernel, n, tp), out_shape=jax.Shap...  62.3 us
    unnamed x5, local copies, waits for them, and re-layouts  2.34 us

profile of v1, /device:TPU:0, one launch (start us, length us, event | category | flops | bytes accessed | tf_op | source)
XLA Modules:
  0.0 65.9 jit_solution(1158410988014489212)
XLA Ops:
  0.0 0.0 copy-start
  0.0 0.7 %copy-done = bf16[2048]{0:T(1024)(128)(2,1)S(1)} copy-done((bf16[2048]{0:T(1024)(128)(2,1)S(1)}, bf16[2048]{0:T(1024)(128)(2,1)}, u32[]{:S(2)}) %copy-start) | copy-done | bytes 4120
  0.7 0.0 copy-start.1
  0.7 0.6 broadcast_in_dim.9.pre_gain
  1.3 0.1 copy-done.1
  1.4 0.6 broadcast_in_dim.11.head_gain
  2.0 62.3 %shard_map.109 = bf16[32,2048]{1,0:T(8,128)(2,1)} custom-call(bf16[32,2048]{1,0:T(8,128)(2,1)} %tokens.1, bf16[1,2048]{1,0:T(2,128)(2,1)} %broadcast_in_dim.9.pre_gain, bf16[256,256]{1,0:T(8,128)(2,1)} %w_key.1, bf16[256,512]{1,0:T(8,128)(2,1)} %w_value.1, bf16[256,256]{1,0:T(8,128)(2,1)} %w_query.1, bf16[8,2048]{1,0:T(8,128)(2,1)} %bitcast.4, ...), custom_call_target="tpu_custom_call" | custom-call | tf_op jit(solution)/shard_map/pallas_call | solution.py:851
  64.3 1.6 %copy.13 = bf16[32,2048]{1,0:T(8,128)(2,1)} copy(bf16[32,2048]{1,0:T(8,128)(2,1)} %shard_map.109) | data formatting | bytes 262144
Async XLA Ops:
  0.0 0.7 %copy-start = (bf16[2048]{0:T(1024)(128)(2,1)S(1)}, bf16[2048]{0:T(1024)(128)(2,1)}, u32[]{:S(2)}) copy-start(bf16[2048]{0:T(1024)(128)(2,1)} %param.12) | copy-start | bytes 12292
  0.7 0.7 %copy-start.1 = (bf16[2048]{0:T(1024)(128)(2,1)S(1)}, bf16[2048]{0:T(1024)(128)(2,1)}, u32[]{:S(2)}) copy-start(bf16[2048]{0:T(1024)(128)(2,1)} %param.20) | copy-start | bytes 12292

commit v2 on v1

--- a/solution.py
+++ b/solution.py
@@ -407,7 +407,7 @@
 
     started = []
 
-    def send(source, target, send_sem, recv_sem, to, flag=None, keep=None):
+    def plan(source, target, send_sem, recv_sem, to, flag=None):
         copy = pltpu.make_async_remote_copy(
             src_ref=source,
             dst_ref=target,
@@ -416,6 +416,10 @@
             device_id={"sp": to[0], "tp": to[1]},
             device_id_type=MESH,
         )
+        started.append((flag, copy))
+        return copy
+
+    def send(source, target, send_sem, recv_sem, to, flag=None, keep=None):
         if keep is not None:
 
             @pl.when(keep)
@@ -423,15 +427,11 @@
                 pltpu.make_async_copy(source, target, recv_sem).start()
 
             flag = jnp.logical_not(keep)
+        copy = plan(source, target, send_sem, recv_sem, to, flag)
         if flag is None:
             copy.start()
         else:
-
-            @pl.when(flag)
-            def _():
-                copy.start()
-
-        started.append((flag, copy))
+            pl.when(flag)(copy.start)
 
     def arrived(target, sem):
         pltpu.make_async_copy(target, target, sem).wait()
@@ -455,94 +455,9 @@
             flag=near,
         )
 
-    layer_a = 2 * c + zl
-    layer_b = 2 * c + flip(zl)
-
-    def first_send(p):
-        _, own, full = pieces[p]
-        for j in range(2):
-            loads_own[p][j].wait()
-        send(
-            own.at[zl],
-            full.at[s],
-            w_send.at[p, 0],
-            w_recv.at[p, s],
-            dev(layer_a, x, y, zh),
-            flag=far,
-        )
-        send(
-            own.at[flip(zl)],
-            full.at[s],
-            w_send.at[p, 1],
-            w_recv.at[p, s],
-            dev(layer_b, x, y, zh),
-        )
-
-    def pass_on(p, block, i, across):
-        _, _, full = pieces[p]
-        sem = w_recv.at[p, block]
-        arrived(full.at[block], sem)
-        if across:
-            send(full.at[block], full.at[block], w_send.at[p, 2 + i], sem, dev(z, flip(x), y, c))
-        send(full.at[block], full.at[block], w_send.at[p, 4 + i], sem, dev(z, x, y, flip(c)))
-
-    block_a = 2 * layer_a + x
-    block_b = 2 * layer_b + x
-    cross_a = 2 * layer_a + flip(x)
-    cross_b = 2 * layer_b + flip(x)
-
-    def pass_first(p, which):
-        pass_on(p, (block_a, block_b)[which], which, True)
-
-    def pass_cross(p):
-        pass_on(p, cross_a, 2, False)
-        pass_on(p, cross_b, 3, False)
-
-    for p in range(3):
-        first_send(p)
-
-    def out_chunk(zb, xb, cb, i):
-        return out_all.at[zb, xb, cb, pl.ds(i * chunk, chunk)]
-
-    def out_pass(zb, xb, i, base, to):
-        for k, target in enumerate(to):
-            part_ref = out_chunk(zb, xb, c, i)
-            send(
-                part_ref,
-                part_ref,
-                out_send.at[base + k, i],
-                out_recv.at[zb, xb, c, i],
-                target,
-            )
-
-    to_x = dev(z, flip(x), y, c)
-    to_core = dev(z, x, y, flip(c))
-    to_half = dev(at_layer(2), x, y, c)
-
-    def token_pass(parity, c_src, i, onward):
-        slot = token_slot(parity, 2 * y + c_src)
-        arrived(slot, tok_recv.at[parity, 0, c_src])
-        if onward:
-            send(
-                slot,
-                slot,
-                tok_send.at[4 + i],
-                tok_recv.at[parity, 0, c_src],
-                dev(at_layer(1), x, y, c),
-                flag=far,
-            )
-        send(
-            slot,
-            slot,
-            tok_send.at[6 + i],
-            tok_recv.at[parity, 1, c_src],
-            dev(z, x, flip(y), c),
-            flag=far if onward else None,
-        )
-
     for copy in loads_small:
         copy.wait()
-    gain = gain_in[...].astype(f32)
+    gain = gain_in[...].astype(f32)[None, :]
 
     def normalize(parity, to_t):
         start = pl.multiple_of((parity * tp + to_t) * rows, rows)
@@ -550,51 +465,152 @@
         scale = lax.rsqrt(jnp.mean(wide * wide, axis=1, keepdims=True) + norm_floor)
         normed[pl.ds(start, rows), :] = (wide * scale * gain).astype(bf16)
 
-    for c_src in range(2):
-        token_pass(zl, c_src, c_src, True)
-    for c_src in range(2):
-        token_pass(flip(zl), c_src, 2 + c_src, False)
-    for copy in loads_out:
-        copy.wait()
-    for i in range(2):
-        out_pass(zh, x, i, 0, (to_x, to_core))
-    pass_first(0, 0)
-    pass_first(0, 1)
+    to_x = dev(z, flip(x), y, c)
+    to_core = dev(z, x, y, flip(c))
+    to_half = dev(at_layer(2), x, y, c)
+
+    def plan_first(p):
+        _, own, full = pieces[p]
+        sem = w_recv.at[p, s]
+        middle = dev(1 + c * (layers - 3), x, y, c)
+        end = dev(c * (layers - 1), x, y, c)
+        beside = dev(at_layer(1), x, y, c)
+        target = full.at[s]
+        return (
+            plan(own.at[flip(c)], target, w_send.at[p, 0], sem, middle, far),
+            plan(own.at[c], target, w_send.at[p, 1], sem, end, far),
+            plan(own.at[flip(zl)], target, w_send.at[p, 1], sem, beside, near),
+        )
+
+    def plan_pass(p, dz, across):
+        block = 2 * at_layer(dz) + (flip(x) if across else x)
+        full = pieces[p][2].at[block]
+        sem = w_recv.at[p, block]
+        i = (10 if across else 6) + dz
+        onward = [plan(full, full, w_send.at[p, i], sem, to_core, near)]
+        if not across:
+            onward.insert(0, plan(full, full, w_send.at[p, 2 + dz], sem, to_x, near))
+
+        def run():
+            arrived(full, sem)
+            for copy in onward:
+                copy.start()
+
+        return run
+
+    def plan_token(parity, c_src, i, onward):
+        slot = token_slot(parity, 2 * y + c_src)
+        sem = tok_recv.at[parity, 0, c_src]
+        out_sem = tok_recv.at[parity, 1, c_src]
+        to_y = dev(z, x, flip(y), c)
+        copies = []
+        if onward:
+            copies.append(
+                plan(slot, slot, tok_send.at[4 + i], sem, dev(at_layer(1), x, y, c), far)
+            )
+        copies.append(
+            plan(slot, slot, tok_send.at[6 + i], out_sem, to_y, far if onward else None)
+        )
+
+        def run(forward=True):
+            arrived(slot, sem)
+            if forward:
+                for copy in copies:
+                    copy.start()
+
+        return run
+
+    def out_chunk(zb, xb, cb, i):
+        return out_all.at[zb, xb, cb, pl.ds(i * chunk, chunk)]
+
+    def plan_out(zb, xb, i, base, to):
+        piece = out_chunk(zb, xb, c, i)
+        sem = out_recv.at[zb, xb, c, i]
+        return [
+            plan(piece, piece, out_send.at[base + k, i], sem, target)
+            for k, target in enumerate(to)
+        ]
+
+    firsts = [plan_first(p) for p in range(3)]
+    direct = [[plan_pass(p, dz, False) for dz in range(layers)] for p in range(3)]
+    cross = [[plan_pass(p, dz, True) for dz in range(layers)] for p in range(3)]
+    token_a = [plan_token(zl, k, k, True) for k in range(2)]
+    token_b = [plan_token(flip(zl), k, 2 + k, False) for k in range(2)]
+    out_own = [plan_out(zh, x, i, 0, (to_x, to_core)) for i in range(2)]
+    out_half = [plan_out(zh, x, i, 2, (to_half,))[0] for i in range(2)]
+
+    out_near_x = [plan_out(zh, flip(x), i, 3, (to_core,)) for i in range(2)]
+    out_far = [plan_out(flip(zh), x, i, 4, (to_x, to_core)) for i in range(2)]
+    out_far_x = [plan_out(flip(zh), flip(x), i, 6, (to_core,)) for i in range(2)]
+
+    def out_from_x():
+        for i in range(2):
+            arrived(out_chunk(zh, flip(x), c, i), out_recv.at[zh, flip(x), c, i])
+            out_near_x[i][0].start()
+
+    def out_from_half():
+        for i in range(2):
+            arrived(out_chunk(flip(zh), x, c, i), out_recv.at[flip(zh), x, c, i])
+            for copy in out_far[i]:
+                copy.start()
+
+    def out_start():
+        for copy in loads_out:
+            copy.wait()
+        for pair in out_own:
+            for copy in pair:
+                copy.start()
+
+    for p in range(3):
+        for j in range(2):
+            loads_own[p][j].wait()
+
+    @pl.when(near)
+    def _():
+        firsts[0][2].start()
+        for p in range(3):
+            direct[p][0]()
+        out_start()
+        for run in token_a:
+            run(False)
+        for run in token_b:
+            run()
+
+    @pl.when(far)
+    def _():
+        for copy in firsts[0][:2]:
+            copy.start()
+        out_start()
+        for run in token_a:
+            run()
+        for i in range(2):
+            firsts[1][i].start()
+        for i in range(2):
+            firsts[2][i].start()
+        for copy in out_half:
+            copy.start()
+        for run in token_b:
+            run()
+
     for parity in range(2):
         for c_src in range(2):
             normalize(parity, 2 * y + c_src)
-    pass_cross(0)
-    pass_first(1, 0)
-    pass_first(1, 1)
+
+    @pl.when(near)
+    def _():
+        direct[0][1]()
+        firsts[1][2].start()
+        firsts[2][2].start()
+        for dz in range(2, layers):
+            direct[0][dz]()
+        for p in range(3):
+            cross[p][0]()
+
     for parity in range(2):
         for c_src in range(2):
             to_t = 2 * flip(y) + c_src
             arrived(token_slot(parity, to_t), tok_recv.at[parity, 1, c_src])
             normalize(parity, to_t)
-
-    cols = (slice(0, dk), slice(dk, dk + dv), slice(dk + dv, 2 * dk + dv))
-    direct = (block_a, block_b, cross_a, cross_b)
-    relayed = [2 * (2 * flip(c) + k) + xx for k in range(2) for xx in range(2)]
-
-    def product(p, block, fresh):
-        at = pl.ds(pl.multiple_of(block * depth, depth), depth)
-        term = jnp.dot(normed[:, at], pieces[p][2][block], preferred_element_type=f32)
-        acc[:, cols[p]] = term if fresh else acc[:, cols[p]] + term
-
-    def direct_products(p):
-        for i, block in enumerate(direct):
-            product(p, block, i == 0)
-
-    def relayed_products(p):
-        for block in relayed:
-            arrived(pieces[p][2].at[block], w_recv.at[p, block])
-            product(p, block, False)
-
-    direct_products(0)
-    pass_cross(1)
-    for i in range(2):
-        out_pass(zh, x, i, 2, (to_half,))
-    relayed_products(0)
 
     all_normed = normed[...]
     gate_in = dot_nt(all_normed, igate_in[...])
@@ -628,12 +644,42 @@
         decay = jnp.where(causal, jnp.exp(log_pair - peak), 0.0)
         gates.append((b_col, total, top, write_scale, peak, decay))
 
-    pass_first(2, 0)
-    pass_first(2, 1)
-    direct_products(1)
-    relayed_products(1)
-    pass_cross(2)
-
+
+    @pl.when(near)
+    def _():
+        direct[1][1]()
+        for dz in range(1, layers):
+            cross[0][dz]()
+        for dz in range(2, layers):
+            direct[1][dz]()
+
+    cols = (slice(0, dk), slice(dk, dk + dv), slice(dk + dv, 2 * dk + dv))
+
+    def products(p):
+        first = True
+        for xx in (x, flip(x)):
+            for dz in range(layers):
+                block = 2 * at_layer(dz) + xx
+                full = pieces[p][2].at[block]
+                pl.when(far)(functools.partial(arrived, full, w_recv.at[p, block]))
+                at = pl.ds(pl.multiple_of(block * depth, depth), depth)
+                term = jnp.dot(normed[:, at], full[...], preferred_element_type=f32)
+                acc[:, cols[p]] = term if first else acc[:, cols[p]] + term
+                first = False
+
+    products(0)
+
+    @pl.when(near)
+    def _():
+        direct[2][1]()
+        for dz in range(1, layers):
+            cross[1][dz]()
+        for dz in range(2, layers):
+            direct[2][dz]()
+        for copy in out_half:
+            copy.start()
+
+    products(1)
     spans = [4 * c + 2 * j + x for j in range(2)]
     keys = (acc[:, cols[0]] * (dk**-0.5)).astype(bf16)
     values = acc[:, cols[1]].astype(bf16)
@@ -677,8 +723,13 @@
                 flag=flag,
             )
 
-    direct_products(2)
-    relayed_products(2)
+    @pl.when(near)
+    def _():
+        for dz in range(1, layers):
+            cross[2][dz]()
+
+    products(2)
+    out_from_half()
     queries = acc[:, cols[2]].astype(bf16)
     intra = []
     for j in range(2):
@@ -689,6 +740,7 @@
         denom = jnp.sum(weights, axis=1, keepdims=True)
         intra.append((numer, denom))
 
+    out_from_x()
     for j in range(2):
         theirs = 4 * c + 2 * j + flip(x)
         arrived(aux_all.at[theirs], aux_recv.at[theirs])
@@ -704,7 +756,7 @@
     top_rows = aux_all[:, 1, :]
     vec_rows = aux_all[:, 2, :]
     place = lax.broadcasted_iota(jnp.int32, span_rows.shape, 0)
-    gain_row = head_gain_in[:, pl.ds(pl.multiple_of(head * dv, dv), dv)].astype(f32)
+    gain_row = head_gain_in[pl.ds(pl.multiple_of(head * dv, dv), dv)].astype(f32)[None, :]
     for j in range(2):
         b_col, total, top, write_scale, peak, decay = gates[j]
         numer, denom = intra[j]
@@ -748,14 +800,8 @@
             )
 
     for i in range(2):
-        arrived(out_chunk(zh, flip(x), c, i), out_recv.at[zh, flip(x), c, i])
-        out_pass(zh, flip(x), i, 3, (to_core,))
-    for i in range(2):
-        arrived(out_chunk(flip(zh), x, c, i), out_recv.at[flip(zh), x, c, i])
-        out_pass(flip(zh), x, i, 4, (to_x, to_core))
-    for i in range(2):
         arrived(out_chunk(flip(zh), flip(x), c, i), out_recv.at[flip(zh), flip(x), c, i])
-        out_pass(flip(zh), flip(x), i, 6, (to_core,))
+        out_far_x[i][0].start()
     for zb in range(2):
         for xb in range(2):
             for i in range(2):
@@ -797,10 +843,7 @@
         if flag is None:
             copy.wait_send()
         else:
-
-            @pl.when(flag)
-            def _():
-                copy.wait_send()
+            pl.when(flag)(copy.wait_send)
 
 
 def on_device_layers(
@@ -857,11 +900,11 @@
             vmem((rows, width), bf16),
             vmem((2 * span, width), bf16),
             vmem((2 * span, width), bf16),
-            vmem((1, width), bf16),
+            vmem((width,), bf16),
             vmem((heads, width), bf16),
             vmem((heads, width), bf16),
             vmem((1, heads), f32),
-            vmem((1, heads * dv), bf16),
+            vmem((heads * dv,), bf16),
             vmem((3, heads, span), f32),
             vmem((2, depth, dk), bf16),
             vmem((2, depth, dv), bf16),
@@ -882,7 +925,7 @@
             dma((2, 2, 2)),
             dma((3,)),
             dma((2,)),
-            dma((3, 8)),
+            dma((3, 6 + 2 * layers)),
             dma((3, n)),
             dma((7, 2)),
             dma((2, 2, 2, 2)),
@@ -898,7 +941,7 @@
         compiler_params=pltpu.CompilerParams(collective_id=0, has_side_effects=True),
     )(
         tokens,
-        pre_gain[None, :],
+        pre_gain,
         w_key,
         w_value,
         w_query,
@@ -906,7 +949,7 @@
         w_fgate.T,
         forget_bias[None, :],
         gate_drift.T,
-        head_gain[None, :],
+        head_gain,
         w_out,
     )
 

time: 67.2 us -> 54 us (0.80)
  Pallas kernels: 62.3 us -> 51.8 us
  local copies, waits for them, and re-layouts: 3.55 us -> 1.57 us
    pallas_call x1, Pallas kernels: 62.3 us -> 51.8 us  [on_device_layers(): pl.pallas_call(functools.partial(layer_kernel, n, tp), out_shape=jax.Shap...]
    broadcast_in_dim x2 -> x0, local copies, waits for them, and re-layouts: 1.21 us -> none  [the longest x1 0.6 us: on_device_layers(): pre_gain[None, :]]
    unnamed x5 -> x1, local copies, waits for them, and re-layouts: 2.34 us -> 1.57 us
where the time goes in v2:
time: 54 us; the launch traced here: 53.3 us
  Pallas kernels  51.8 us (96%)
  local copies, waits for them, and re-layouts  1.57 us (3%)
    pallas_call x1, Pallas kernels, on_device_layers(): pl.pallas_call(functools.partial(layer_kernel, n, tp), out_shape=jax.Shap...  51.8 us
    unnamed x1, local copies, waits for them, and re-layouts  1.57 us

profile of v2, /device:TPU:0, one launch (start us, length us, event | category | flops | bytes accessed | tf_op | source)
XLA Modules:
  0.0 53.3 jit_solution(4301463041833991998)
XLA Ops:
  0.0 51.8 %shard_map.109 = bf16[32,2048]{1,0:T(8,128)(2,1)} custom-call(bf16[32,2048]{1,0:T(8,128)(2,1)} %tokens.1, bf16[2048]{0:T(1024)(128)(2,1)} %pre_gain.1, bf16[256,256]{1,0:T(8,128)(2,1)} %w_key.1, bf16[256,512]{1,0:T(8,128)(2,1)} %w_value.1, bf16[256,256]{1,0:T(8,128)(2,1)} %w_query.1, bf16[8,2048]{1,0:T(8,128)(2,1)} %bitcast.4, bf16[8,2048]{1,0:T(8,128)(2,1)} %bitcast.5, ...), custom_call_target="tpu_custom_call" | custom-call | tf_op jit(solution)/shard_map/pallas_call | solution.py:894
  51.8 1.6 %copy.13 = bf16[32,2048]{1,0:T(8,128)(2,1)} copy(bf16[32,2048]{1,0:T(8,128)(2,1)} %shard_map.109) | data formatting | bytes 262144

commit v3 on v2

--- a/solution.py
+++ b/solution.py
@@ -270,7 +270,6 @@
     heads,
     heads_in,
     part,
-    final_in,
     load_sems,
     tok_send,
     tok_recv,
@@ -548,11 +547,10 @@
             arrived(out_chunk(zh, flip(x), c, i), out_recv.at[zh, flip(x), c, i])
             out_near_x[i][0].start()
 
-    def out_from_half():
-        for i in range(2):
-            arrived(out_chunk(flip(zh), x, c, i), out_recv.at[flip(zh), x, c, i])
-            for copy in out_far[i]:
-                copy.start()
+    def out_from_half(i):
+        arrived(out_chunk(flip(zh), x, c, i), out_recv.at[flip(zh), x, c, i])
+        for copy in out_far[i]:
+            copy.start()
 
     def out_start():
         for copy in loads_out:
@@ -567,8 +565,8 @@
 
     @pl.when(near)
     def _():
-        firsts[0][2].start()
-        for p in range(3):
+        firsts[1][2].start()
+        for p in (1, 0, 2):
             direct[p][0]()
         out_start()
         for run in token_a:
@@ -578,15 +576,14 @@
 
     @pl.when(far)
     def _():
-        for copy in firsts[0][:2]:
-            copy.start()
+        firsts[1][1].start()
+        firsts[1][0].start()
         out_start()
         for run in token_a:
             run()
-        for i in range(2):
-            firsts[1][i].start()
-        for i in range(2):
-            firsts[2][i].start()
+        for p in (0, 2):
+            for i in (1, 0):
+                firsts[p][i].start()
         for copy in out_half:
             copy.start()
         for run in token_b:
@@ -598,12 +595,12 @@
 
     @pl.when(near)
     def _():
-        direct[0][1]()
-        firsts[1][2].start()
+        firsts[0][2].start()
         firsts[2][2].start()
+        direct[1][1]()
         for dz in range(2, layers):
-            direct[0][dz]()
-        for p in range(3):
+            direct[1][dz]()
+        for p in (1, 0, 2):
             cross[p][0]()
 
     for parity in range(2):
@@ -647,39 +644,37 @@
 
     @pl.when(near)
     def _():
-        direct[1][1]()
         for dz in range(1, layers):
-            cross[0][dz]()
-        for dz in range(2, layers):
-            direct[1][dz]()
-
-    cols = (slice(0, dk), slice(dk, dk + dv), slice(dk + dv, 2 * dk + dv))
-
-    def products(p):
-        first = True
-        for xx in (x, flip(x)):
-            for dz in range(layers):
-                block = 2 * at_layer(dz) + xx
-                full = pieces[p][2].at[block]
-                pl.when(far)(functools.partial(arrived, full, w_recv.at[p, block]))
-                at = pl.ds(pl.multiple_of(block * depth, depth), depth)
-                term = jnp.dot(normed[:, at], full[...], preferred_element_type=f32)
-                acc[:, cols[p]] = term if first else acc[:, cols[p]] + term
-                first = False
-
-    products(0)
-
-    @pl.when(near)
-    def _():
-        direct[2][1]()
+            direct[0][dz]()
         for dz in range(1, layers):
             cross[1][dz]()
-        for dz in range(2, layers):
+        for dz in range(1, layers):
             direct[2][dz]()
         for copy in out_half:
             copy.start()
 
+    cols = (slice(0, dk), slice(dk, dk + dv), slice(dk + dv, 2 * dk + dv))
+
+    def products(p):
+        full = pieces[p][2]
+
+        @pl.when(far)
+        def _():
+            for block in range(n):
+                arrived(full.at[block], w_recv.at[p, block])
+
+        flat = full[...].reshape(n * depth, full.shape[2])
+        acc[:, cols[p]] = jnp.dot(normed[...], flat, preferred_element_type=f32)
+
     products(1)
+
+    @pl.when(near)
+    def _():
+        for dz in range(1, layers):
+            cross[0][dz]()
+
+    products(0)
+
     spans = [4 * c + 2 * j + x for j in range(2)]
     keys = (acc[:, cols[0]] * (dk**-0.5)).astype(bf16)
     values = acc[:, cols[1]].astype(bf16)
@@ -729,7 +724,6 @@
             cross[2][dz]()
 
     products(2)
-    out_from_half()
     queries = acc[:, cols[2]].astype(bf16)
     intra = []
     for j in range(2):
@@ -740,7 +734,7 @@
         denom = jnp.sum(weights, axis=1, keepdims=True)
         intra.append((numer, denom))
 
-    out_from_x()
+    out_from_half(0)
     for j in range(2):
         theirs = 4 * c + 2 * j + flip(x)
         arrived(aux_all.at[theirs], aux_recv.at[theirs])
@@ -799,45 +793,65 @@
                 keep=near & (zl == d) & (c == j),
             )
 
-    for i in range(2):
-        arrived(out_chunk(flip(zh), flip(x), c, i), out_recv.at[flip(zh), flip(x), c, i])
-        out_far_x[i][0].start()
-    for zb in range(2):
+    out_from_x()
+    out_from_half(1)
+    features = out_all.shape[3]
+    home = 2 * zh + c
+    wide = 2 * features
+
+    def landing(yy, zz, zb):
+        start = pl.multiple_of((zz + 2 * zb) * wide, wide)
+        return out.at[yy, :, pl.ds(start, wide)]
+
+    def out_arrived(zb):
         for xb in range(2):
             for i in range(2):
                 arrived(out_chunk(zb, xb, flip(c), i), out_recv.at[zb, xb, flip(c), i])
-    for m in range(layers):
-        arrived(heads_in.at[m], heads_recv.at[m])
-
-    features = out_all.shape[3]
-    home = 2 * zh + c
-    for zb in range(2):
-        for xb in range(2):
-            total = jnp.zeros((span, features), f32)
-            for m in range(layers):
-                total = total + dot_nt(
-                    heads_in[m], out_all[zb, xb, m // 2, :, (m % 2) * dv : (m % 2 + 1) * dv]
-                )
-            part[zb, :, xb * features : (xb + 1) * features] = total.astype(bf16)
+
+    def heads_arrived(half):
+        for i in range(2):
+            arrived(heads_in.at[2 * half + i], heads_recv.at[2 * half + i])
+
+    def project(zb, xb, half):
+        total = jnp.zeros((span, features), f32)
+        for i in range(2):
+            total = total + dot_nt(
+                heads_in[2 * half + i], out_all[zb, xb, half, :, i * dv : (i + 1) * dv]
+            )
+        return total
+
+    def share(zb):
         for yy in range(2):
             for cc in range(2):
                 send(
                     part.at[zb, pl.ds((2 * yy + cc) * rows, rows)],
-                    final_in.at[zl, y, zb],
+                    landing(y, zl, zb),
                     final_send.at[zb, yy, cc],
                     final_recv.at[zl, y, zb],
                     dev(home, x, yy, cc),
                     keep=(zl == c) & (y == yy) & (c == cc),
                 )
-    wide = 2 * features
+
+    out_arrived(zh)
+    heads_arrived(zh)
+    early_part = [project(zh, xb, zh) for xb in range(2)]
+    for i in range(2):
+        arrived(out_chunk(flip(zh), flip(x), c, i), out_recv.at[flip(zh), flip(x), c, i])
+        out_far_x[i][0].start()
+    heads_arrived(flip(zh))
+    for xb in range(2):
+        total = early_part[xb] + project(zh, xb, flip(zh))
+        part[zh, :, xb * features : (xb + 1) * features] = total.astype(bf16)
+    share(zh)
+    out_arrived(flip(zh))
+    for xb in range(2):
+        total = project(flip(zh), xb, zh) + project(flip(zh), xb, flip(zh))
+        part[flip(zh), :, xb * features : (xb + 1) * features] = total.astype(bf16)
+    share(flip(zh))
     for zb in range(2):
         for zz in range(2):
-            total = jnp.zeros((rows, wide), f32)
             for yy in range(2):
-                arrived(final_in.at[zz, yy, zb], final_recv.at[zz, yy, zb])
-                total = total + final_in[zz, yy, zb].astype(f32)
-            at = (zz + 2 * zb) * wide
-            out[:, at : at + wide] = total.astype(bf16)
+                arrived(landing(yy, zz, zb), final_recv.at[zz, yy, zb])
 
     for flag, copy in started:
         if flag is None:
@@ -891,11 +905,11 @@
     anywhere = pl.BlockSpec(memory_space=pl.ANY)
     dma = pltpu.SemaphoreType.DMA
     vmem = pltpu.VMEM
-    return pl.pallas_call(
+    parts = pl.pallas_call(
         functools.partial(layer_kernel, n, tp),
-        out_shape=jax.ShapeDtypeStruct((rows, features * n), bf16),
+        out_shape=pltpu.VMEM((2, rows, features * n), bf16),
         in_specs=[anywhere] * 11,
-        out_specs=pl.BlockSpec(memory_space=pltpu.VMEM),
+        out_specs=anywhere,
         scratch_shapes=[
             vmem((rows, width), bf16),
             vmem((2 * span, width), bf16),
@@ -919,7 +933,6 @@
             vmem((2, span, dv), bf16),
             vmem((layers, span, dv), bf16),
             vmem((2, span, 2 * features), bf16),
-            vmem((2, 2, 2, rows, 2 * features), bf16),
             dma((15,)),
             dma((10,)),
             dma((2, 2, 2)),
@@ -952,6 +965,7 @@
         head_gain,
         w_out,
     )
+    return jnp.sum(parts.astype(f32), axis=0).astype(bf16)
 
 
 def solution(mesh):

time: 54 us -> 51.2 us (0.948)
  local copies, waits for them, and re-layouts: 1.57 us -> 0 us
  Pallas kernels: 51.8 us -> 50.3 us
  other arithmetic: 0 us -> 0.71 us
    unnamed x1 -> x0, local copies, waits for them, and re-layouts: 1.57 us -> none
    pallas_call x1, Pallas kernels: 51.8 us -> 50.3 us  [on_device_layers(): pl.pallas_call(functools.partial(layer_kernel, n, tp), out_shape=pltpu.VM...]
    reduce_sum x0 -> x1, other arithmetic: none -> 0.71 us  [on_device_layers(): return jnp.sum(parts.astype(f32), axis=0).astype(bf16)]
where the time goes in v3:
time: 51.2 us; the launch traced here: 51 us
  Pallas kernels  50.3 us (98%)
  other arithmetic  0.71 us (1%)
    pallas_call x1, Pallas kernels, on_device_layers(): pl.pallas_call(functools.partial(layer_kernel, n, tp), out_shape=pltpu.VM...  50.3 us

profile of v3, /device:TPU:0, one launch (start us, length us, event | category | flops | bytes accessed | tf_op | source)
XLA Modules:
  0.0 51.0 jit_solution(3347748121387501817)
XLA Ops:
  0.0 50.3 %shard_map.109 = bf16[2,32,2048]{2,1,0:T(8,128)(2,1)S(1)} custom-call(bf16[32,2048]{1,0:T(8,128)(2,1)} %tokens.1, bf16[2048]{0:T(1024)(128)(2,1)} %pre_gain.1, bf16[256,256]{1,0:T(8,128)(2,1)} %w_key.1, bf16[256,512]{1,0:T(8,128)(2,1)} %w_value.1, bf16[256,256]{1,0:T(8,128)(2,1)} %w_query.1, bf16[8,2048]{1,0:T(8,128)(2,1)} %bitcast.4, ...), custom_call_target="tpu_custom_call" | custom-call | tf_op jit(solution)/shard_map/pallas_call | solution.py:908
  50.3 0.7 %reduce_sum.12 = bf16[32,2048]{1,0:T(8,128)(2,1)} reduce(bf16[2,32,2048]{2,1,0:T(8,128)(2,1)S(1)} %shard_map.109, bf16[]{:T(256)} %constant.2.clone.1), dimensions={0}, to_apply=%region_0.0 | reduce | flops 65536 | bytes 393218 | tf_op jit(solution)/shard_map/reduce_sum | solution.py:968

commit v4 on v3

--- a/solution.py
+++ b/solution.py
@@ -347,7 +347,7 @@
                 load(
                     w_hbm.at[:, pl.ds(j * width, width)],
                     own.at[j],
-                    load_sems.at[1 + 2 * p + j],
+                    load_sems.at[1 + p],
                 )
                 for j in range(2)
             ]
@@ -357,7 +357,7 @@
         load(
             w_out.at[pl.ds(i * chunk, chunk)],
             out_all.at[zh, x, c, pl.ds(i * chunk, chunk)],
-            load_sems.at[7 + i],
+            load_sems.at[4],
         )
         for i in range(2)
     ]
@@ -368,7 +368,7 @@
         (forget_bias, bias_in),
         (head_gain, head_gain_in),
     )
-    loads_small = [load(a, b, load_sems.at[9 + i]) for i, (a, b) in enumerate(small)]
+    loads_small = [load(a, b, load_sems.at[5 + i]) for i, (a, b) in enumerate(small)]
 
     @pl.when(near)
     def _():
@@ -384,7 +384,7 @@
                         w_hbm.at[:, pl.ds(j * width, width)], full.at[s], w_recv.at[p, s]
                     ).start()
 
-    load_drift = load(drift, drift_in.at[2], load_sems.at[14])
+    load_drift = load(drift, drift_in.at[2], load_sems.at[10])
 
     barrier = pltpu.get_barrier_semaphore()
     me = s * tp + t
@@ -404,8 +404,6 @@
 
     pl.semaphore_wait(barrier, n * tp - 1)
 
-    started = []
-
     def plan(source, target, send_sem, recv_sem, to, flag=None):
         copy = pltpu.make_async_remote_copy(
             src_ref=source,
@@ -415,7 +413,6 @@
             device_id={"sp": to[0], "tp": to[1]},
             device_id_type=MESH,
         )
-        started.append((flag, copy))
         return copy
 
     def send(source, target, send_sem, recv_sem, to, flag=None, keep=None):
@@ -438,17 +435,17 @@
     load_tokens.wait()
     mine = tok_recv.at[zl, 0, c]
     send(tok_own, own_slot, tok_send.at[0], mine, dev(at_layer(2), x, y, zh))
-    send(tok_own, own_slot, tok_send.at[1], mine, dev(at_layer(1), x, y, zh))
+    send(tok_own, own_slot, tok_send.at[0], mine, dev(at_layer(1), x, y, zh))
     send(
-        tok_own, own_slot, tok_send.at[2], tok_recv.at[zl, 1, c], dev(z, x, flip(y), zh)
-    )
-    send(tok_own, own_slot, tok_send.at[3], mine, dev(z, x, y, flip(c)), flag=far)
+        tok_own, own_slot, tok_send.at[0], tok_recv.at[zl, 1, c], dev(z, x, flip(y), zh)
+    )
+    send(tok_own, own_slot, tok_send.at[0], mine, dev(z, x, y, flip(c)), flag=far)
     load_drift.wait()
     for i in range(1, 4):
         send(
             drift_in.at[2],
             drift_in.at[zl],
-            drift_send.at[i - 1],
+            drift_send.at[0],
             drift_recv.at[zl],
             dev(at_layer(i), x, y, c),
             flag=near,
@@ -477,18 +474,18 @@
         target = full.at[s]
         return (
             plan(own.at[flip(c)], target, w_send.at[p, 0], sem, middle, far),
-            plan(own.at[c], target, w_send.at[p, 1], sem, end, far),
-            plan(own.at[flip(zl)], target, w_send.at[p, 1], sem, beside, near),
+            plan(own.at[c], target, w_send.at[p, 0], sem, end, far),
+            plan(own.at[flip(zl)], target, w_send.at[p, 0], sem, beside, near),
         )
 
     def plan_pass(p, dz, across):
         block = 2 * at_layer(dz) + (flip(x) if across else x)
         full = pieces[p][2].at[block]
         sem = w_recv.at[p, block]
-        i = (10 if across else 6) + dz
-        onward = [plan(full, full, w_send.at[p, i], sem, to_core, near)]
+        to_far = w_recv.at[p, 0]
+        onward = [plan(full, full, w_send.at[p, 2], to_far, to_core, near)]
         if not across:
-            onward.insert(0, plan(full, full, w_send.at[p, 2 + dz], sem, to_x, near))
+            onward.insert(0, plan(full, full, w_send.at[p, 1], sem, to_x, near))
 
         def run():
             arrived(full, sem)
@@ -505,10 +502,10 @@
         copies = []
         if onward:
             copies.append(
-                plan(slot, slot, tok_send.at[4 + i], sem, dev(at_layer(1), x, y, c), far)
+                plan(slot, slot, tok_send.at[1], sem, dev(at_layer(1), x, y, c), far)
             )
         copies.append(
-            plan(slot, slot, tok_send.at[6 + i], out_sem, to_y, far if onward else None)
+            plan(slot, slot, tok_send.at[1], out_sem, to_y, far if onward else None)
         )
 
         def run(forward=True):
@@ -522,46 +519,46 @@
     def out_chunk(zb, xb, cb, i):
         return out_all.at[zb, xb, cb, pl.ds(i * chunk, chunk)]
 
-    def plan_out(zb, xb, i, base, to):
+    def plan_out(zb, xb, i, to):
         piece = out_chunk(zb, xb, c, i)
-        sem = out_recv.at[zb, xb, c, i]
-        return [
-            plan(piece, piece, out_send.at[base + k, i], sem, target)
-            for k, target in enumerate(to)
-        ]
+        targets = {
+            "half": (out_send.at[0], out_recv.at[i], to_half),
+            "x": (out_send.at[1], out_recv.at[2], to_x),
+            "far_x": (out_send.at[1], out_recv.at[3 + i], to_x),
+            "core": (out_send.at[2], out_recv.at[5 + zb], to_core),
+        }
+        return [plan(piece, piece, targets[k][0], targets[k][1], targets[k][2]) for k in to]
 
     firsts = [plan_first(p) for p in range(3)]
     direct = [[plan_pass(p, dz, False) for dz in range(layers)] for p in range(3)]
     cross = [[plan_pass(p, dz, True) for dz in range(layers)] for p in range(3)]
     token_a = [plan_token(zl, k, k, True) for k in range(2)]
     token_b = [plan_token(flip(zl), k, 2 + k, False) for k in range(2)]
-    out_own = [plan_out(zh, x, i, 0, (to_x, to_core)) for i in range(2)]
-    out_half = [plan_out(zh, x, i, 2, (to_half,))[0] for i in range(2)]
-
-    out_near_x = [plan_out(zh, flip(x), i, 3, (to_core,)) for i in range(2)]
-    out_far = [plan_out(flip(zh), x, i, 4, (to_x, to_core)) for i in range(2)]
-    out_far_x = [plan_out(flip(zh), flip(x), i, 6, (to_core,)) for i in range(2)]
+    out_own = [plan_out(zh, x, i, ("x", "core")) for i in range(2)]
+    out_half = [plan_out(zh, x, i, ("half",))[0] for i in range(2)]
+
+    out_near_x = [plan_out(zh, flip(x), i, ("core",)) for i in range(2)]
+    out_far = [plan_out(flip(zh), x, i, ("far_x", "core")) for i in range(2)]
+    out_far_x = [plan_out(flip(zh), flip(x), i, ("core",)) for i in range(2)]
 
     def out_from_x():
+        arrived(out_all.at[zh, flip(x), c], out_recv.at[2])
         for i in range(2):
-            arrived(out_chunk(zh, flip(x), c, i), out_recv.at[zh, flip(x), c, i])
             out_near_x[i][0].start()
 
     def out_from_half(i):
-        arrived(out_chunk(flip(zh), x, c, i), out_recv.at[flip(zh), x, c, i])
+        arrived(out_chunk(flip(zh), x, c, i), out_recv.at[i])
         for copy in out_far[i]:
             copy.start()
 
     def out_start():
-        for copy in loads_out:
-            copy.wait()
+        arrived(out_all.at[zh, x, c], load_sems.at[4])
         for pair in out_own:
             for copy in pair:
                 copy.start()
 
     for p in range(3):
-        for j in range(2):
-            loads_own[p][j].wait()
+        arrived(pieces[p][1], load_sems.at[1 + p])
 
     @pl.when(near)
     def _():
@@ -581,13 +578,16 @@
         out_start()
         for run in token_a:
             run()
-        for p in (0, 2):
-            for i in (1, 0):
-                firsts[p][i].start()
+        for i in (1, 0):
+            firsts[0][i].start()
+        arrived(pieces[0][1], w_send.at[0, 0])
+        for i in (1, 0):
+            firsts[2][i].start()
+        for run in token_b:
+            run()
+        arrived(pieces[2][1], w_send.at[2, 0])
         for copy in out_half:
             copy.start()
-        for run in token_b:
-            run()
 
     for parity in range(2):
         for c_src in range(2):
@@ -660,8 +660,7 @@
 
         @pl.when(far)
         def _():
-            for block in range(n):
-                arrived(full.at[block], w_recv.at[p, block])
+            arrived(full, w_recv.at[p, 0])
 
         flat = full[...].reshape(n * depth, full.shape[2])
         acc[:, cols[p]] = jnp.dot(normed[...], flat, preferred_element_type=f32)
@@ -699,21 +698,22 @@
             (dev(z, x, y, flip(c)), early),
         )
     ):
+        group = 0 if k == 0 else 1
         for j in range(2):
             mine = spans[j]
             send(
                 aux_all.at[mine],
                 aux_all.at[mine],
-                aux_send.at[k, j],
-                aux_recv.at[mine],
+                aux_send.at[0],
+                aux_recv.at[group],
                 to,
                 flag=flag,
             )
             send(
                 state_all.at[mine],
                 state_all.at[mine],
-                state_send.at[k, j],
-                state_recv.at[mine],
+                state_send.at[0],
+                state_recv.at[group],
                 to,
                 flag=flag,
             )
@@ -734,17 +734,14 @@
         denom = jnp.sum(weights, axis=1, keepdims=True)
         intra.append((numer, denom))
 
-    out_from_half(0)
-    for j in range(2):
-        theirs = 4 * c + 2 * j + flip(x)
-        arrived(aux_all.at[theirs], aux_recv.at[theirs])
-        arrived(state_all.at[theirs], state_recv.at[theirs])
+    pl.when(near)(functools.partial(out_from_half, 0))
+    arrived(aux_all.at[pl.ds(0, 2)], aux_recv.at[0])
+    arrived(state_all.at[pl.ds(0, 2)], state_recv.at[0])
 
     @pl.when(late)
     def _():
-        for m in range(layers):
-            arrived(aux_all.at[m], aux_recv.at[m])
-            arrived(state_all.at[m], state_recv.at[m])
+        arrived(aux_all.at[pl.ds(0, layers)], aux_recv.at[1])
+        arrived(state_all.at[pl.ds(0, layers)], state_recv.at[1])
 
     span_rows = aux_all[:, 0, :]
     top_rows = aux_all[:, 1, :]
@@ -787,13 +784,14 @@
             send(
                 heads.at[j],
                 heads_in.at[z],
-                heads_send.at[j, d],
-                heads_recv.at[z],
+                heads_send.at[0],
+                heads_recv.at[zh],
                 dev(2 * c + d, x, y, j),
                 keep=near & (zl == d) & (c == j),
             )
 
     out_from_x()
+    pl.when(far)(functools.partial(out_from_half, 0))
     out_from_half(1)
     features = out_all.shape[3]
     home = 2 * zh + c
@@ -804,13 +802,10 @@
         return out.at[yy, :, pl.ds(start, wide)]
 
     def out_arrived(zb):
-        for xb in range(2):
-            for i in range(2):
-                arrived(out_chunk(zb, xb, flip(c), i), out_recv.at[zb, xb, flip(c), i])
+        arrived(out_all.at[zb, :, flip(c)], out_recv.at[5 + zb])
 
     def heads_arrived(half):
-        for i in range(2):
-            arrived(heads_in.at[2 * half + i], heads_recv.at[2 * half + i])
+        arrived(heads_in.at[pl.ds(2 * half, 2)], heads_recv.at[half])
 
     def project(zb, xb, half):
         total = jnp.zeros((span, features), f32)
@@ -826,8 +821,8 @@
                 send(
                     part.at[zb, pl.ds((2 * yy + cc) * rows, rows)],
                     landing(y, zl, zb),
-                    final_send.at[zb, yy, cc],
-                    final_recv.at[zl, y, zb],
+                    final_send.at[0],
+                    final_recv.at[0],
                     dev(home, x, yy, cc),
                     keep=(zl == c) & (y == yy) & (c == cc),
                 )
@@ -836,7 +831,7 @@
     heads_arrived(zh)
     early_part = [project(zh, xb, zh) for xb in range(2)]
     for i in range(2):
-        arrived(out_chunk(flip(zh), flip(x), c, i), out_recv.at[flip(zh), flip(x), c, i])
+        arrived(out_chunk(flip(zh), flip(x), c, i), out_recv.at[3 + i])
         out_far_x[i][0].start()
     heads_arrived(flip(zh))
     for xb in range(2):
@@ -848,16 +843,37 @@
         total = project(flip(zh), xb, zh) + project(flip(zh), xb, flip(zh))
         part[flip(zh), :, xb * features : (xb + 1) * features] = total.astype(bf16)
     share(flip(zh))
-    for zb in range(2):
-        for zz in range(2):
-            for yy in range(2):
-                arrived(landing(yy, zz, zb), final_recv.at[zz, yy, zb])
-
-    for flag, copy in started:
+    arrived(out, final_recv.at[0])
+
+    def drained(ref, sem, flag=None):
         if flag is None:
-            copy.wait_send()
+            arrived(ref, sem)
         else:
-            pl.when(flag)(copy.wait_send)
+            pl.when(flag)(functools.partial(arrived, ref, sem))
+
+    drained(tok_all.at[pl.ds(0, 4 * rows)], tok_send.at[0], far)
+    drained(tok_all.at[pl.ds(0, 6 * rows)], tok_send.at[1], far)
+    drained(tok_all.at[pl.ds(0, 3 * rows)], tok_send.at[0], near)
+    drained(tok_all.at[pl.ds(0, 2 * rows)], tok_send.at[1], near)
+    drained(drift_in, drift_send.at[0], near)
+    for p in range(3):
+        _, own, full = pieces[p]
+        if p == 1:
+            drained(own, w_send.at[p, 0], far)
+        drained(own.at[0], w_send.at[p, 0], near)
+        drained(full.at[pl.ds(0, layers)], w_send.at[p, 1], near)
+        drained(full, w_send.at[p, 2], near)
+    drained(out_all.at[0, 0, 0], out_send.at[0])
+    drained(out_all.at[0, 0], out_send.at[1])
+    drained(out_all.at[0], out_send.at[2])
+    for ref, sem in ((state_all, state_send.at[0]), (aux_all, aux_send.at[0])):
+        drained(ref.at[pl.ds(0, 6)], sem, early)
+        drained(ref.at[pl.ds(0, 2)], sem, late)
+    drained(heads_in.at[pl.ds(0, 3)], heads_send.at[0], near)
+    drained(heads_in, heads_send.at[0], far)
+    at_home = zl == c
+    drained(part, final_send.at[0], jnp.logical_not(at_home))
+    drained(part.at[:, pl.ds(0, 3 * rows)], final_send.at[0], at_home)
 
 
 def on_device_layers(
@@ -933,23 +949,23 @@
             vmem((2, span, dv), bf16),
             vmem((layers, span, dv), bf16),
             vmem((2, span, 2 * features), bf16),
-            dma((15,)),
-            dma((10,)),
+            dma((11,)),
+            dma((2,)),
             dma((2, 2, 2)),
+            dma((1,)),
+            dma((2,)),
+            dma((3, 3)),
+            dma((3, n)),
             dma((3,)),
+            dma((7,)),
+            dma((1,)),
             dma((2,)),
-            dma((3, 6 + 2 * layers)),
-            dma((3, n)),
-            dma((7, 2)),
-            dma((2, 2, 2, 2)),
-            dma((3, 2)),
-            dma((n,)),
-            dma((3, 2)),
-            dma((n,)),
-            dma((2, 2)),
-            dma((layers,)),
-            dma((2, 2, 2)),
-            dma((2, 2, 2)),
+            dma((1,)),
+            dma((2,)),
+            dma((1,)),
+            dma((2,)),
+            dma((1,)),
+            dma((1,)),
         ],
         compiler_params=pltpu.CompilerParams(collective_id=0, has_side_effects=True),
     )(

time: 51.2 us -> 48.9 us (0.955)
  Pallas kernels: 50.3 us -> 48.1 us
    pallas_call x1, Pallas kernels: 50.3 us -> 48.1 us  [on_device_layers(): pl.pallas_call(functools.partial(layer_kernel, n, tp), out_shape=pltpu.VM...]
where the time goes in v4:
time: 48.9 us; the launch traced here: 48.8 us
  Pallas kernels  48.1 us (98%)
  other arithmetic  0.71 us (1%)
    pallas_call x1, Pallas kernels, on_device_layers(): pl.pallas_call(functools.partial(layer_kernel, n, tp), out_shape=pltpu.VM...  48.1 us

profile of v4, /device:TPU:0, one launch (start us, length us, event | category | flops | bytes accessed | tf_op | source)
XLA Modules:
  0.0 48.8 jit_solution(9689302815144133563)
XLA Ops:
  0.0 48.1 %shard_map.109 = bf16[2,32,2048]{2,1,0:T(8,128)(2,1)S(1)} custom-call(bf16[32,2048]{1,0:T(8,128)(2,1)} %tokens.1, bf16[2048]{0:T(1024)(128)(2,1)} %pre_gain.1, bf16[256,256]{1,0:T(8,128)(2,1)} %w_key.1, bf16[256,512]{1,0:T(8,128)(2,1)} %w_value.1, bf16[256,256]{1,0:T(8,128)(2,1)} %w_query.1, bf16[8,2048]{1,0:T(8,128)(2,1)} %bitcast.4, ...), custom_call_target="tpu_custom_call" | custom-call | tf_op jit(solution)/shard_map/pallas_call | solution.py:924
  48.1 0.7 %reduce_sum.12 = bf16[32,2048]{1,0:T(8,128)(2,1)} reduce(bf16[2,32,2048]{2,1,0:T(8,128)(2,1)S(1)} %shard_map.109, bf16[]{:T(256)} %constant.2.clone.1), dimensions={0}, to_apply=%region_0.0 | reduce | flops 65536 | bytes 393218 | tf_op jit(solution)/shard_map/reduce_sum | solution.py:984

commit v5 on v4

--- a/solution.py
+++ b/solution.py
@@ -322,6 +322,21 @@
     def dev(zz, xx, yy, cc):
         return 2 * zz + xx, 2 * yy + cc
 
+    barrier = pltpu.get_barrier_semaphore()
+    to_sibling = dev(z, x, y, flip(c))
+    partners = [dev(z, flip(x), y, cc) for cc in range(2)]
+    for dz in range(layers):
+        for yy in (y, flip(y)) if dz < 2 else (y,):
+            partners += [dev(at_layer(dz), x, yy, cc) for cc in range(2)]
+    partners[2:4] = [to_sibling]
+    for ss, tt in partners:
+        pl.semaphore_signal(
+            barrier,
+            inc=1,
+            device_id={"sp": ss, "tp": tt},
+            device_id_type=MESH,
+        )
+
     def load(source, target, sem):
         copy = pltpu.make_async_copy(source, target, sem)
         copy.start()
@@ -386,23 +401,12 @@
 
     load_drift = load(drift, drift_in.at[2], load_sems.at[10])
 
-    barrier = pltpu.get_barrier_semaphore()
-    me = s * tp + t
-    for i in range(1, n * tp):
-        other = lax.rem(me + i, n * tp)
-        pl.semaphore_signal(
-            barrier,
-            inc=1,
-            device_id={"sp": other // tp, "tp": lax.rem(other, tp)},
-            device_id_type=MESH,
-        )
-
     @pl.when(c == 0)
     def _():
         state_all[layers:, :, :] = jnp.zeros((layers, dk, dv), bf16)
         aux_all[layers:, :, :] = jnp.zeros((layers, aux_all.shape[1], dk), f32)
 
-    pl.semaphore_wait(barrier, n * tp - 1)
+    pl.semaphore_wait(barrier, len(partners))
 
     def plan(source, target, send_sem, recv_sem, to, flag=None):
         copy = pltpu.make_async_remote_copy(
@@ -525,7 +529,7 @@
             "half": (out_send.at[0], out_recv.at[i], to_half),
             "x": (out_send.at[1], out_recv.at[2], to_x),
             "far_x": (out_send.at[1], out_recv.at[3 + i], to_x),
-            "core": (out_send.at[2], out_recv.at[5 + zb], to_core),
+            "core": (out_send.at[2], out_recv.at[5 + 2 * zb + xb], to_core),
         }
         return [plan(piece, piece, targets[k][0], targets[k][1], targets[k][2]) for k in to]
 
@@ -575,16 +579,16 @@
     def _():
         firsts[1][1].start()
         firsts[1][0].start()
+        firsts[0][1].start()
+        firsts[0][0].start()
         out_start()
         for run in token_a:
             run()
         for i in (1, 0):
-            firsts[0][i].start()
-        arrived(pieces[0][1], w_send.at[0, 0])
-        for i in (1, 0):
             firsts[2][i].start()
         for run in token_b:
             run()
+        arrived(pieces[0][1], w_send.at[0, 0])
         arrived(pieces[2][1], w_send.at[2, 0])
         for copy in out_half:
             copy.start()
@@ -797,12 +801,12 @@
     home = 2 * zh + c
     wide = 2 * features
 
-    def landing(yy, zz, zb):
-        start = pl.multiple_of((zz + 2 * zb) * wide, wide)
-        return out.at[yy, :, pl.ds(start, wide)]
-
-    def out_arrived(zb):
-        arrived(out_all.at[zb, :, flip(c)], out_recv.at[5 + zb])
+    def landing(yy, zz, zb, xb):
+        start = pl.multiple_of((zz + 2 * zb) * wide + xb * features, features)
+        return out.at[yy, :, pl.ds(start, features)]
+
+    def out_arrived(zb, xb):
+        arrived(out_all.at[zb, xb, flip(c)], out_recv.at[5 + 2 * zb + xb])
 
     def heads_arrived(half):
         arrived(heads_in.at[pl.ds(2 * half, 2)], heads_recv.at[half])
@@ -815,34 +819,33 @@
             )
         return total
 
-    def share(zb):
+    def share(zb, xb, total):
+        part[zb, xb] = total.astype(bf16)
         for yy in range(2):
             for cc in range(2):
                 send(
-                    part.at[zb, pl.ds((2 * yy + cc) * rows, rows)],
-                    landing(y, zl, zb),
+                    part.at[zb, xb, pl.ds((2 * yy + cc) * rows, rows)],
+                    landing(y, zl, zb, xb),
                     final_send.at[0],
                     final_recv.at[0],
                     dev(home, x, yy, cc),
                     keep=(zl == c) & (y == yy) & (c == cc),
                 )
 
-    out_arrived(zh)
+    sides = (x, flip(x))
+    for xb in sides:
+        out_arrived(zh, xb)
     heads_arrived(zh)
-    early_part = [project(zh, xb, zh) for xb in range(2)]
+    early_part = [project(zh, xb, zh) for xb in sides]
     for i in range(2):
         arrived(out_chunk(flip(zh), flip(x), c, i), out_recv.at[3 + i])
         out_far_x[i][0].start()
     heads_arrived(flip(zh))
-    for xb in range(2):
-        total = early_part[xb] + project(zh, xb, flip(zh))
-        part[zh, :, xb * features : (xb + 1) * features] = total.astype(bf16)
-    share(zh)
-    out_arrived(flip(zh))
-    for xb in range(2):
-        total = project(flip(zh), xb, zh) + project(flip(zh), xb, flip(zh))
-        part[flip(zh), :, xb * features : (xb + 1) * features] = total.astype(bf16)
-    share(flip(zh))
+    for k, xb in enumerate(sides):
+        share(zh, xb, early_part[k] + project(zh, xb, flip(zh)))
+    for xb in sides:
+        out_arrived(flip(zh), xb)
+        share(flip(zh), xb, project(flip(zh), xb, zh) + project(flip(zh), xb, flip(zh)))
     arrived(out, final_recv.at[0])
 
     def drained(ref, sem, flag=None):
@@ -873,7 +876,7 @@
     drained(heads_in, heads_send.at[0], far)
     at_home = zl == c
     drained(part, final_send.at[0], jnp.logical_not(at_home))
-    drained(part.at[:, pl.ds(0, 3 * rows)], final_send.at[0], at_home)
+    drained(part.at[:, :, pl.ds(0, 3 * rows)], final_send.at[0], at_home)
 
 
 def on_device_layers(
@@ -948,7 +951,7 @@
             vmem((n, 8, dk), f32),
             vmem((2, span, dv), bf16),
             vmem((layers, span, dv), bf16),
-            vmem((2, span, 2 * features), bf16),
+            vmem((2, 2, span, features), bf16),
             dma((11,)),
             dma((2,)),
             dma((2, 2, 2)),
@@ -957,7 +960,7 @@
             dma((3, 3)),
             dma((3, n)),
             dma((3,)),
-            dma((7,)),
+            dma((9,)),
             dma((1,)),
             dma((2,)),
             dma((1,)),

time: 48.9 us -> 47.6 us (0.973)
  Pallas kernels: 48.1 us -> 46.8 us
    pallas_call x1, Pallas kernels: 48.1 us -> 46.8 us  [on_device_layers(): pl.pallas_call(functools.partial(layer_kernel, n, tp), out_shape=pltpu.VM...]
where the time goes in v5:
time: 47.6 us; the launch traced here: 47.5 us
  Pallas kernels  46.8 us (98%)
  other arithmetic  0.71 us (1%)
    pallas_call x1, Pallas kernels, on_device_layers(): pl.pallas_call(functools.partial(layer_kernel, n, tp), out_shape=pltpu.VM...  46.8 us

profile of v5, /device:TPU:0, one launch (start us, length us, event | category | flops | bytes accessed | tf_op | source)
XLA Modules:
  0.0 47.5 jit_solution(16597618312556082984)
XLA Ops:
  0.0 46.8 %shard_map.109 = bf16[2,32,2048]{2,1,0:T(8,128)(2,1)S(1)} custom-call(bf16[32,2048]{1,0:T(8,128)(2,1)} %tokens.1, bf16[2048]{0:T(1024)(128)(2,1)} %pre_gain.1, bf16[256,256]{1,0:T(8,128)(2,1)} %w_key.1, bf16[256,512]{1,0:T(8,128)(2,1)} %w_value.1, bf16[256,256]{1,0:T(8,128)(2,1)} %w_query.1, bf16[8,2048]{1,0:T(8,128)(2,1)} %bitcast.4, ...), custom_call_target="tpu_custom_call" | custom-call | tf_op jit(solution)/shard_map/pallas_call | solution.py:927
  46.8 0.7 %reduce_sum.12 = bf16[32,2048]{1,0:T(8,128)(2,1)} reduce(bf16[2,32,2048]{2,1,0:T(8,128)(2,1)S(1)} %shard_map.109, bf16[]{:T(256)} %constant.2.clone.1), dimensions={0}, to_apply=%region_0.0 | reduce | flops 65536 | bytes 393218 | tf_op jit(solution)/shard_map/reduce_sum | solution.py:987

commit v6 on v5

--- a/solution.py
+++ b/solution.py
@@ -276,6 +276,7 @@
     drift_send,
     drift_recv,
     w_send,
+    pass_send,
     w_recv,
     out_send,
     out_recv,
@@ -388,7 +389,7 @@
     @pl.when(near)
     def _():
         pltpu.make_async_copy(tokens, own_slot, tok_recv.at[zl, 0, c]).start()
-        pltpu.make_async_copy(drift, drift_in.at[zl], drift_recv.at[zl]).start()
+        pltpu.make_async_copy(drift, drift_in.at[zl], drift_recv.at[0]).start()
         for p, (w_hbm, own, full) in enumerate(pieces):
             width = own.shape[2]
             for j in range(2):
@@ -396,7 +397,7 @@
                 @pl.when(zl == j)
                 def _():
                     pltpu.make_async_copy(
-                        w_hbm.at[:, pl.ds(j * width, width)], full.at[s], w_recv.at[p, s]
+                        w_hbm.at[:, pl.ds(j * width, width)], full.at[s], w_recv.at[p, 0]
                     ).start()
 
     load_drift = load(drift, drift_in.at[2], load_sems.at[10])
@@ -450,7 +451,7 @@
             drift_in.at[2],
             drift_in.at[zl],
             drift_send.at[0],
-            drift_recv.at[zl],
+            drift_recv.at[0],
             dev(at_layer(i), x, y, c),
             flag=near,
         )
@@ -471,28 +472,32 @@
 
     def plan_first(p):
         _, own, full = pieces[p]
-        sem = w_recv.at[p, s]
+        sem = w_recv.at[p, 2]
+        side_sem = w_recv.at[p, 1]
         middle = dev(1 + c * (layers - 3), x, y, c)
         end = dev(c * (layers - 1), x, y, c)
         beside = dev(at_layer(1), x, y, c)
         target = full.at[s]
         return (
-            plan(own.at[flip(c)], target, w_send.at[p, 0], sem, middle, far),
-            plan(own.at[c], target, w_send.at[p, 0], sem, end, far),
-            plan(own.at[flip(zl)], target, w_send.at[p, 0], sem, beside, near),
-        )
-
-    def plan_pass(p, dz, across):
-        block = 2 * at_layer(dz) + (flip(x) if across else x)
-        full = pieces[p][2].at[block]
-        sem = w_recv.at[p, block]
+            plan(own.at[flip(c)], target, w_send.at[p], sem, middle, far),
+            plan(own.at[c], target, w_send.at[p], sem, end, far),
+            plan(own.at[flip(zl)], target, w_send.at[p], side_sem, beside, near),
+        )
+
+    def plan_pass(p, dzs, across):
+        blocks = [2 * at_layer(dz) + (flip(x) if across else x) for dz in dzs]
+        refs = [pieces[p][2].at[block] for block in blocks]
+        sem = w_recv.at[p, (3 if dzs[0] == 0 else 4) if across else min(dzs[0], 2)]
+        across_sem = w_recv.at[p, 3 if dzs[0] == 0 else 4]
         to_far = w_recv.at[p, 0]
-        onward = [plan(full, full, w_send.at[p, 2], to_far, to_core, near)]
-        if not across:
-            onward.insert(0, plan(full, full, w_send.at[p, 1], sem, to_x, near))
+        onward = []
+        for full in refs:
+            if not across:
+                onward.append(plan(full, full, pass_send.at[0], across_sem, to_x, near))
+            onward.append(plan(full, full, pass_send.at[1], to_far, to_core, near))
 
         def run():
-            arrived(full, sem)
+            arrived(pieces[p][2].at[pl.ds(0, len(refs))], sem)
             for copy in onward:
                 copy.start()
 
@@ -534,8 +539,8 @@
         return [plan(piece, piece, targets[k][0], targets[k][1], targets[k][2]) for k in to]
 
     firsts = [plan_first(p) for p in range(3)]
-    direct = [[plan_pass(p, dz, False) for dz in range(layers)] for p in range(3)]
-    cross = [[plan_pass(p, dz, True) for dz in range(layers)] for p in range(3)]
+    direct = [[plan_pass(p, dzs, False) for dzs in ((0,), (1,), (2, 3))] for p in range(3)]
+    cross = [[plan_pass(p, dzs, True) for dzs in ((0,), (1, 2, 3))] for p in range(3)]
     token_a = [plan_token(zl, k, k, True) for k in range(2)]
     token_b = [plan_token(flip(zl), k, 2 + k, False) for k in range(2)]
     out_own = [plan_out(zh, x, i, ("x", "core")) for i in range(2)]
@@ -588,8 +593,8 @@
             firsts[2][i].start()
         for run in token_b:
             run()
-        arrived(pieces[0][1], w_send.at[0, 0])
-        arrived(pieces[2][1], w_send.at[2, 0])
+        arrived(pieces[0][1], w_send.at[0])
+        arrived(pieces[2][1], w_send.at[2])
         for copy in out_half:
             copy.start()
 
@@ -602,8 +607,7 @@
         firsts[0][2].start()
         firsts[2][2].start()
         direct[1][1]()
-        for dz in range(2, layers):
-            direct[1][dz]()
+        direct[1][2]()
         for p in (1, 0, 2):
             cross[p][0]()
 
@@ -625,9 +629,9 @@
     col_id = lax.broadcasted_iota(jnp.int32, (span, span), 1)
     causal = row_id >= col_id
     eye = row_id == col_id
+    arrived(drift_in.at[pl.ds(0, 2)], drift_recv.at[0])
     gates = []
     for j in range(2):
-        arrived(drift_in.at[j], drift_recv.at[j])
         offset = drift_in[j, pl.ds(head, 1), :][:, :1]
         pre = forget_all[j * span : (j + 1) * span] + offset
         in_col = input_all[j * span : (j + 1) * span]
@@ -648,12 +652,11 @@
 
     @pl.when(near)
     def _():
-        for dz in range(1, layers):
-            direct[0][dz]()
-        for dz in range(1, layers):
-            cross[1][dz]()
-        for dz in range(1, layers):
-            direct[2][dz]()
+        direct[0][1]()
+        direct[0][2]()
+        cross[1][1]()
+        direct[2][1]()
+        direct[2][2]()
         for copy in out_half:
             copy.start()
 
@@ -673,8 +676,7 @@
 
     @pl.when(near)
     def _():
-        for dz in range(1, layers):
-            cross[0][dz]()
+        cross[0][1]()
 
     products(0)
 
@@ -724,8 +726,7 @@
 
     @pl.when(near)
     def _():
-        for dz in range(1, layers):
-            cross[2][dz]()
+        cross[2][1]()
 
     products(2)
     queries = acc[:, cols[2]].astype(bf16)
@@ -862,10 +863,10 @@
     for p in range(3):
         _, own, full = pieces[p]
         if p == 1:
-            drained(own, w_send.at[p, 0], far)
-        drained(own.at[0], w_send.at[p, 0], near)
-        drained(full.at[pl.ds(0, layers)], w_send.at[p, 1], near)
-        drained(full, w_send.at[p, 2], near)
+            drained(own, w_send.at[p], far)
+        drained(own.at[0], w_send.at[p], near)
+    drained(out_all.at[0], pass_send.at[0], near)
+    drained(out_all, pass_send.at[1], near)
     drained(out_all.at[0, 0, 0], out_send.at[0])
     drained(out_all.at[0, 0], out_send.at[1])
     drained(out_all.at[0], out_send.at[2])
@@ -956,9 +957,10 @@
             dma((2,)),
             dma((2, 2, 2)),
             dma((1,)),
+            dma((1,)),
+            dma((3,)),
             dma((2,)),
-            dma((3, 3)),
-            dma((3, n)),
+            dma((3, 5)),
             dma((3,)),
             dma((9,)),
             dma((1,)),

time: 47.6 us -> 47.4 us (level)
  no operation moved by 1% of the time
where the time goes in v6:
time: 47.4 us; the launch traced here: 47.1 us
  Pallas kernels  46.4 us (98%)
  other arithmetic  0.71 us (1%)
    pallas_call x1, Pallas kernels, on_device_layers(): pl.pallas_call(functools.partial(layer_kernel, n, tp), out_shape=pltpu.VM...  46.4 us

profile of v6, /device:TPU:0, one launch (start us, length us, event | category | flops | bytes accessed | tf_op | source)
XLA Modules:
  0.0 47.1 jit_solution(17835784085991795820)
XLA Ops:
  0.0 46.4 %shard_map.109 = bf16[2,32,2048]{2,1,0:T(8,128)(2,1)S(1)} custom-call(bf16[32,2048]{1,0:T(8,128)(2,1)} %tokens.1, bf16[2048]{0:T(1024)(128)(2,1)} %pre_gain.1, bf16[256,256]{1,0:T(8,128)(2,1)} %w_key.1, bf16[256,512]{1,0:T(8,128)(2,1)} %w_value.1, bf16[256,256]{1,0:T(8,128)(2,1)} %w_query.1, bf16[8,2048]{1,0:T(8,128)(2,1)} %bitcast.4, ...), custom_call_target="tpu_custom_call" | custom-call | tf_op jit(solution)/shard_map/pallas_call | solution.py:928
  46.4 0.7 %reduce_sum.12 = bf16[32,2048]{1,0:T(8,128)(2,1)} reduce(bf16[2,32,2048]{2,1,0:T(8,128)(2,1)S(1)} %shard_map.109, bf16[]{:T(256)} %constant.2.clone.1), dimensions={0}, to_apply=%region_0.0 | reduce | flops 65536 | bytes 393218 | tf_op jit(solution)/shard_map/reduce_sum | solution.py:989

commit v7 on v6

--- a/solution.py
+++ b/solution.py
@@ -594,9 +594,9 @@
         for run in token_b:
             run()
         arrived(pieces[0][1], w_send.at[0])
-        arrived(pieces[2][1], w_send.at[2])
         for copy in out_half:
             copy.start()
+        arrived(pieces[2][1], w_send.at[2])
 
     for parity in range(2):
         for c_src in range(2):

time: 47.4 us -> 47.4 us (level)
  no operation moved by 1% of the time
where the time goes in v7:
time: 47.4 us; the launch traced here: 47.1 us
  Pallas kernels  46.4 us (98%)
  other arithmetic  0.71 us (1%)
    pallas_call x1, Pallas kernels, on_device_layers(): pl.pallas_call(functools.partial(layer_kernel, n, tp), out_shape=pltpu.VM...  46.4 us

profile of v7, /device:TPU:0, one launch (start us, length us, event | category | flops | bytes accessed | tf_op | source)
XLA Modules:
  0.0 47.1 jit_solution(11647176795452030022)
XLA Ops:
  0.0 46.4 %shard_map.109 = bf16[2,32,2048]{2,1,0:T(8,128)(2,1)S(1)} custom-call(bf16[32,2048]{1,0:T(8,128)(2,1)} %tokens.1, bf16[2048]{0:T(1024)(128)(2,1)} %pre_gain.1, bf16[256,256]{1,0:T(8,128)(2,1)} %w_key.1, bf16[256,512]{1,0:T(8,128)(2,1)} %w_value.1, bf16[256,256]{1,0:T(8,128)(2,1)} %w_query.1, bf16[8,2048]{1,0:T(8,128)(2,1)} %bitcast.4, ...), custom_call_target="tpu_custom_call" | custom-call | tf_op jit(solution)/shard_map/pallas_call | solution.py:928
  46.4 0.7 %reduce_sum.12 = bf16[32,2048]{1,0:T(8,128)(2,1)} reduce(bf16[2,32,2048]{2,1,0:T(8,128)(2,1)S(1)} %shard_map.109, bf16[]{:T(256)} %constant.2.clone.1), dimensions={0}, to_apply=%region_0.0 | reduce | flops 65536 | bytes 393218 | tf_op jit(solution)/shard_map/reduce_sum | solution.py:989
